TPU v7x, 32 devices: a whole 2x2x4 slice. The times are simulated.
32 devices in a mesh: rep: 2 (over x), fs: 8 (over z, y), tp: 2 (over core).
Axes of the slice: x: 2, y: 2, z: 4, core: 2. Of those that a mesh axis runs over, the one named last changes fastest.
Arguments:
- tokens: bfloat16 [10240, 2048], P(('rep', 'fs'), 'tp'), may hold values from -6 to 6
- norm_first: float32 [2048], replicated, may hold values from 0.1 to 1.9
- norm_mix: float32 [2048], replicated, may hold values from 0.1 to 1.9
- norm_second: float32 [2048], replicated, may hold values from 0.1 to 1.9
- gate_weight: float32 [2048, 2816], P('fs', 'tp'), may hold values from -0.125 to 0.125
- up_weight: float32 [2048, 2816], P('fs', 'tp'), may hold values from -0.125 to 0.125
- down_weight: float32 [2816, 2048], P('tp', 'fs'), may hold values from -0.109375 to 0.109375
- gate_scale: float32 [2816], P('tp'), may hold values from 0.3 to 3
- up_scale: float32 [2816], P('tp'), may hold values from 0.3 to 3
- down_scale: float32 [2048], P('fs'), may hold values from 0.3 to 3
- u_weight: float32 [2048, 1024], P('fs', 'tp'), may hold values from -0.125 to 0.125
- v_weight: float32 [2048, 1024], P('fs', 'tp'), may hold values from -0.125 to 0.125
- u_scale: float32 [1024], P('tp'), may hold values from 0.3 to 3
- v_scale: float32 [1024], P('tp'), may hold values from 0.15 to 6
- ln_gain: float32 [1024], P('tp'), may hold values from 0.1 to 1.9
- ln_bias: float32 [1024], P('tp'), may hold values from -3 to 3
- spatial_weight: bfloat16 [8, 128, 128], P('tp'), may hold values from -0.25 to 0.25
- spatial_bias: float32 [8, 128], P('tp'), may hold values from 0.1 to 1.9
- out_weight: float32 [1024, 2048], P('tp', 'fs'), may hold values from -0.1875 to 0.1875
- out_scale: float32 [2048], P('fs'), may hold values from 0.3 to 3
Outputs:
- layer_out: bfloat16 [10240, 2048], P(('rep', 'fs'), 'tp')
All inputs are finite; a program needn't handle non-finite values.
Results may differ from a plain program's by a relative error of at most 0.019.
Values may be sent and summed in bfloat16 or wider, within the bound.
No kernel may reach another device: no remote copies, remote signals or barrier semaphores. Data moves between devices by JAX's collectives and lax.ppermute only.
A program may use at most 128 MiB of HBM per device.

v0:
```python
import jax
import jax.numpy as jnp
from jax import lax
from jax.experimental import pallas as pl
from jax.experimental.pallas import tpu as pltpu
from jax.sharding import PartitionSpec as P


EPS = 1e-06
LANES = 128
SPARE = 16
HBM = pl.BlockSpec(memory_space=pltpu.HBM)
VMEM = pl.BlockSpec(memory_space=pltpu.VMEM)
SMEM = pl.BlockSpec(memory_space=pltpu.SMEM)
BF, F32 = jnp.bfloat16, jnp.float32


def params():
    return pltpu.CompilerParams(vmem_limit_bytes=60 * 1024 * 1024)


def cost(flops, size):
    return pl.CostEstimate(flops=flops, bytes_accessed=size, transcendentals=0)


def lane(start):
    return pl.ds(pl.multiple_of(start * LANES, LANES), LANES)


def pack_pairs(left, right, places, stages):
    rows = left.shape[0]

    def body(at, l_ref, r_ref, *outs):
        outs = iter(outs)
        for stage in stages:
            for group in (stage.near, stage.far_z):
                out = next(outs)
                for k, place in enumerate(group):
                    n = at[place]
                    out[0, :, 2 * k * LANES : (2 * k + 1) * LANES] = l_ref[:, lane(n)].astype(BF)
                    out[0, :, (2 * k + 1) * LANES : (2 * k + 2) * LANES] = r_ref[:, lane(n)].astype(BF)

    shapes = [
        jax.ShapeDtypeStruct((1, rows, 2 * LANES * len(group)), BF) for stage in stages for group in (stage.near, stage.far_z)
    ]
    out = pl.pallas_call(
        body,
        out_shape=shapes,
        in_specs=[SMEM, VMEM, VMEM],
        out_specs=[VMEM] * len(shapes),
        compiler_params=params(),
        cost_estimate=cost(1000, 6 * left.size * 2),
    )(places, left, right)
    return [(out[2 * i], out[2 * i + 1]) for i in range(len(stages))]


def pack_rows(weight, scale, places, stage):
    columns = weight.shape[1]

    def body(at, w_ref, s_ref, near_ref, far_ref):
        for k, place in enumerate(stage.near):
            near_ref[0, SPARE + k * LANES : SPARE + (k + 1) * LANES, :] = w_ref[lane(at[place]), :].astype(BF)
        for k, place in enumerate(stage.far_z):
            far_ref[0, k * LANES : (k + 1) * LANES, :] = w_ref[lane(at[place]), :].astype(BF)
        value = s_ref[...]
        high = value.astype(BF)
        rest = value - high.astype(F32)
        mid = rest.astype(BF)
        low = (rest - mid.astype(F32)).astype(BF)
        row = lax.broadcasted_iota(jnp.int32, (SPARE, columns), 0)
        pick = jnp.where(row == 0, high.astype(F32), jnp.where(row == 1, mid.astype(F32), jnp.where(row == 2, low.astype(F32), 0.0)))
        near_ref[0, :SPARE, :] = pick.astype(BF)

    return pl.pallas_call(
        body,
        out_shape=[
            jax.ShapeDtypeStruct((1, len(stage.near) * LANES + SPARE, columns), BF),
            jax.ShapeDtypeStruct((1, len(stage.far_z) * LANES, columns), BF),
        ],
        in_specs=[SMEM, VMEM, VMEM],
        out_specs=[VMEM, VMEM],
        compiler_params=params(),
        cost_estimate=cost(1000, 6 * weight.size),
    )(places, weight, scale.reshape(1, columns))


class Stage:
    def __init__(self, name, tiles, unit, axis, head):
        self.name, self.tiles, self.unit, self.axis, self.head = name, tiles, unit, axis, head
        n = len(tiles)
        self.fz, self.fy = max(1, n // 5), n // 2
        back = list(reversed(tiles))
        self.near, self.far_z = tiles[: n - self.fz], back[: self.fz]
        self.near_y, self.far_y = tiles[: n - self.fy], back[: self.fy]

    def runs(self):
        out = []
        unit, head, fz, fy = self.unit, self.head, self.fz, self.fy

        def put(piece, block, count, offset, tiles, with_head=False):
            at = offset
            if with_head:
                at += head
            k = 0
            while k < len(tiles):
                n = 1
                while k + n < len(tiles) and tiles[k + n] == tiles[k] + n:
                    n += 1
                start, size, place = at + k * unit, n * unit, head + tiles[k] * unit
                if with_head and head and k == 0:
                    if tiles[0] == 0:
                        start, size, place = start - head, size + head, place - head
                    else:
                        out.append((piece, block, count, offset, 0, head))
                out.append((piece, block, count, start, place, size))
                k += n

        put(0, 0, 1, 0, self.near, True)
        put(1, 1, 1, 0, self.near, True)
        put(2, 2, 2, 0, self.near, True)
        put(3, 0, 1, 0, self.far_z)
        put(4, 4, 2, 0, self.near_y, True)
        put(5, 6, 2, 0, self.near_y, True)
        put(6, 1, 1, 0, self.far_z)
        put(6, 4, 1, fz * unit, self.far_y)
        put(6, 5, 1, (fz + fy) * unit, self.far_y)
        put(7, 2, 2, 0, self.far_z)
        put(7, 6, 2, fz * unit, self.far_y)
        return out


N_PIECES = 8


def fetches(stage, pieces, scratch, sems, first):
    out = []
    for piece, block, count, start, place, size in stage.runs():
        if stage.axis == 2:
            source = pieces[piece].at[:, :, pl.ds(start, size)]
            target = scratch.at[pl.ds(block, count), :, pl.ds(place, size)]
        else:
            source = pieces[piece].at[:, pl.ds(start, size), :]
            target = scratch.at[pl.ds(block, count), pl.ds(place, size), :]
        out.append(pltpu.make_async_copy(source, target, sems.at[first + len(out)]))
    return out


def norm_rows(rows, gains):
    values = rows.astype(F32)
    factor = lax.rsqrt(jnp.mean(values * values, axis=1, keepdims=True) + EPS)
    return (values * factor * gains).astype(BF)


def local_gain(gain_ref, at, blocks):
    return jnp.concatenate([gain_ref[pl.ds(at[l], 1), :] for l in range(blocks)], axis=1)


def residual_and_norm(rest, weight, terms, gains, new_ref, normed, step):
    count, _ = rest.shape

    @pl.loop(0, count // step, unroll=4)
    def _(i):
        here = pl.ds(pl.multiple_of(i * step, step), step)
        rows = rest[here, :]
        if terms:
            total = terms[0][here, :].astype(F32) + terms[1][here, :].astype(F32)
            rows = (rows.astype(F32) + weight * total).astype(BF)
            new_ref[here, :] = rows
        normed[here, :] = norm_rows(rows, gains)


def flat(ref, columns):
    block = ref[:, :, columns]
    return block.reshape(block.shape[0] * block.shape[1], block.shape[2])


def hidden_units(config, place, normed, w_up, gs_ref, us_ref, out):
    tiles, chunk = config["tiles"], config["chunk"]

    @pl.loop(0, normed.shape[0] // chunk)
    def _(i):
        here = pl.ds(pl.multiple_of(i * chunk, chunk), chunk)
        lhs = normed[here, :]
        for k in range(tiles):
            rhs = flat(w_up, slice(2 * k * LANES, (2 * k + 2) * LANES))
            acc = jnp.dot(lhs, rhs, preferred_element_type=F32)
            n = place[k]
            gate = acc[:, :LANES] * gs_ref[pl.ds(n, 1), :]
            up_part = acc[:, LANES:] * us_ref[pl.ds(n, 1), :]
            out[here, k * LANES : (k + 1) * LANES] = (gate / (1.0 + jnp.exp(-gate)) * up_part).astype(BF)


def feed_forward(config, ids, state, gain, stages, pieces, scales, last):
    blocks, tiles, chunk, place_of = config["blocks"], config["tiles"], config["chunk"], config["place"]
    count, width = state[0].shape
    columns = width // blocks
    units = tiles * LANES
    n_state = len(state)
    n_copies = sum(len(stage.runs()) for stage in stages)

    def body(*refs):
        at, place, refs = refs[0], refs[1], refs[2:]
        sources, refs = refs[:n_state], refs[n_state:]
        gain_ref, gs_ref, us_ref, refs = refs[0], refs[1], refs[2], refs[3:]
        parts = [refs[N_PIECES * i : N_PIECES * (i + 1)] for i in range(len(stages))]
        refs = refs[N_PIECES * len(stages) :]
        n_out = 3 if last else len(state[:2])
        outs, refs = refs[:n_out], refs[n_out:]
        w_up, w_down, normed, hidden, sems, refs = refs[0], refs[1], refs[2], refs[3], refs[4], refs[5:]
        st, refs = refs[:n_state], refs[n_state:]
        loads = [pltpu.make_async_copy(a, b, sems.at[n_copies + k]) for k, (a, b) in enumerate(zip(sources, st))]
        up = fetches(stages[0], parts[0], w_up, sems, 0)
        up += fetches(stages[1], parts[1], w_up, sems, len(up))
        down = fetches(stages[2], parts[2], w_down, sems, len(up))
        for copy in loads + up + down:
            copy.start()
        gains = local_gain(gain_ref, at, blocks)
        for copy in loads:
            copy.wait()
        residual_and_norm(st[0], 0.5 if not last else 1.0, st[1:], gains, st[0], normed, 16)
        saves = []
        if n_state > 1 and not last:
            saves.append(pltpu.make_async_copy(st[0], outs[1], sems.at[n_copies + 3]))
            saves[0].start()
        for copy in up:
            copy.wait()

        hidden_units(config, place, normed, w_up, gs_ref, us_ref, hidden)

        for copy in down:
            copy.wait()
        halves, rests = refs if last else (refs[0], None)

        @pl.loop(0, count // chunk)
        def _(i):
            here = pl.ds(pl.multiple_of(i * chunk, chunk), chunk)
            left = hidden[here, :]
            for l in range(blocks):
                acc = jnp.dot(left, w_down[l, SPARE:, :], preferred_element_type=F32)
                terms = w_down[l, :SPARE, :].astype(F32)
                value = (acc * (terms[0:1] + terms[1:2] + terms[2:3])).astype(BF)
                block = slice(l * columns, (l + 1) * columns)
                if not last:
                    halves[here, block] = value
                else:
                    j = at[l]
                    side = jnp.where(lax.div(j, blocks // 2) == at[blocks], 0, 1)
                    there = pl.ds(pl.multiple_of(lax.rem(j, blocks // 2) * columns, columns), columns)
                    halves[side, here, there] = value
                    rests[side, here, there] = st[0][here, block]

        if last:
            results = ((halves.at[1], outs[1]), (halves.at[0], outs[0]), (rests.at[0], outs[2]))
        else:
            results = ((halves, outs[0]),)
        results = [pltpu.make_async_copy(a, b, sems.at[n_copies + 4 + k]) for k, (a, b) in enumerate(results)]
        for copy in results:
            copy.start()
        for copy in results + saves:
            copy.wait()

    if last:
        shapes = [jax.ShapeDtypeStruct((count, width // 2), BF)] * 3
        extra = [pltpu.VMEM((2, count, width // 2), BF)] * 2
    else:
        shapes = [jax.ShapeDtypeStruct((count, width), BF)] * len(state[:2])
        extra = [pltpu.VMEM((count, width), BF)]
    return pl.pallas_call(
        body,
        out_shape=shapes,
        in_specs=[SMEM, SMEM] + [HBM] * n_state + [VMEM] * 3 + [HBM] * (N_PIECES * len(stages)),
        out_specs=[HBM] * len(shapes),
        scratch_shapes=[
            pltpu.VMEM((blocks, columns, 2 * units), BF),
            pltpu.VMEM((blocks, SPARE + units, columns), BF),
            pltpu.VMEM((count, width), BF),
            pltpu.VMEM((count, units), BF),
            pltpu.SemaphoreType.DMA((n_copies + 8,)),
        ]
        + [pltpu.VMEM((count, width), BF)] * n_state
        + extra,
        compiler_params=params(),
        cost_estimate=cost(6 * count * width * units, 2 * 3 * width * units),
    )(
        ids,
        place_of,
        *state,
        gain.reshape(blocks, columns),
        scales[0].reshape(tiles, LANES),
        scales[1].reshape(tiles, LANES),
        *[p for group in pieces for p in group],
    )


def first_hidden(config, ids, state, gain, stages, pieces, scales):
    blocks, tiles = config["blocks"], config["tiles"]
    count, width = state.shape
    columns, units = width // blocks, tiles * LANES
    n_copies = sum(len(stage.runs()) for stage in stages)

    def body(at, place, source, gain_ref, gs_ref, us_ref, *refs):
        parts = [refs[N_PIECES * i : N_PIECES * (i + 1)] for i in range(len(stages))]
        out, w_up, normed, sems, st = refs[N_PIECES * len(stages) :]
        load = pltpu.make_async_copy(source, st, sems.at[n_copies])
        up = []
        for stage, part in zip(stages, parts):
            up += fetches(stage, part, w_up, sems, len(up))
        for copy in [load] + up:
            copy.start()
        gains = local_gain(gain_ref, at, blocks)
        load.wait()
        residual_and_norm(st, 0.5, (), gains, None, normed, 16)
        for copy in up:
            copy.wait()
        hidden_units(config, place, normed, w_up, gs_ref, us_ref, out)

    return pl.pallas_call(
        body,
        out_shape=jax.ShapeDtypeStruct((count, units), BF),
        in_specs=[SMEM, SMEM, HBM] + [VMEM] * 3 + [HBM] * (N_PIECES * len(stages)),
        out_specs=VMEM,
        scratch_shapes=[
            pltpu.VMEM((blocks, columns, 2 * units), BF),
            pltpu.VMEM((count, width), BF),
            pltpu.SemaphoreType.DMA((n_copies + 1,)),
            pltpu.VMEM((count, width), BF),
        ],
        compiler_params=params(),
        cost_estimate=cost(4 * count * width * units, 2 * 2 * width * units),
    )(
        ids,
        config["place"],
        state,
        gain.reshape(blocks, columns),
        scales[0].reshape(tiles, LANES),
        scales[1].reshape(tiles, LANES),
        *[p for group in pieces for p in group],
    )


def first_down(config, hidden, stage, pieces):
    blocks, chunk, width = config["blocks"], config["chunk"], config["width"]
    count, units = hidden.shape
    columns = width // blocks
    n_copies = len(stage.runs())

    def body(left_ref, *refs):
        out, w_down, sems = refs[N_PIECES:]
        copies = fetches(stage, refs[:N_PIECES], w_down, sems, 0)
        for copy in copies:
            copy.start()
        for copy in copies:
            copy.wait()

        @pl.loop(0, count // chunk)
        def _(i):
            here = pl.ds(pl.multiple_of(i * chunk, chunk), chunk)
            left = left_ref[here, :]
            for l in range(blocks):
                acc = jnp.dot(left, w_down[l, SPARE:, :], preferred_element_type=F32)
                terms = w_down[l, :SPARE, :].astype(F32)
                out[here, l * columns : (l + 1) * columns] = (acc * (terms[0:1] + terms[1:2] + terms[2:3])).astype(BF)

    return pl.pallas_call(
        body,
        out_shape=jax.ShapeDtypeStruct((count, width), BF),
        in_specs=[VMEM] + [HBM] * N_PIECES,
        out_specs=VMEM,
        scratch_shapes=[pltpu.VMEM((blocks, SPARE + units, columns), BF), pltpu.SemaphoreType.DMA((n_copies,))],
        compiler_params=params(),
        cost_estimate=cost(2 * count * width * units, 2 * width * units),
    )(hidden, *pieces)


def gelu(a):
    return 0.5 * a * (1.0 + jnp.tanh(0.7978845608028654 * (a + 0.044715 * a * a * a)))


def mixer_in(config, ids, state, gain, stage, pieces, scales):
    blocks, tiles, chunk = config["blocks"], config["tiles"], config["chunk"]
    count, width = state[0].shape
    columns = width // blocks
    n_copies = len(stage.runs())

    def body(*refs):
        at, place, refs = refs[0], refs[1], refs[2:]
        sources, gain_ref, us_ref, vs_ref = refs[:3], refs[3], refs[4], refs[5]
        parts, refs = refs[6 : 6 + N_PIECES], refs[6 + N_PIECES :]
        new_out, u_out, v_out, sum_out, w, normed, sems, *st = refs
        loads = [pltpu.make_async_copy(a, b, sems.at[n_copies + k]) for k, (a, b) in enumerate(zip(sources, st))]
        copies = fetches(stage, parts, w, sems, 0)
        for copy in loads + copies:
            copy.start()
        gains = local_gain(gain_ref, at, blocks)
        for copy in loads:
            copy.wait()
        residual_and_norm(st[0], 0.5, st[1:], gains, st[0], normed, 16)
        save = pltpu.make_async_copy(st[0], new_out, sems.at[n_copies + 3])
        save.start()
        for copy in copies:
            copy.wait()

        @pl.loop(0, count // chunk)
        def _(i):
            here = pl.ds(pl.multiple_of(i * chunk, chunk), chunk)
            lhs = normed[here, :]
            plain = jnp.zeros((chunk, LANES), F32)
            square = jnp.zeros((chunk, LANES), F32)
            for k in range(tiles):
                rhs = flat(w, slice(2 * k * LANES, (2 * k + 2) * LANES))
                acc = jnp.dot(lhs, rhs, preferred_element_type=F32)
                n = place[k]
                block = slice(k * LANES, (k + 1) * LANES)
                u_out[here, block] = gelu(acc[:, :LANES] * us_ref[pl.ds(n, 1), :])
                v_act = gelu(acc[:, LANES:] * vs_ref[pl.ds(n, 1), :])
                v_out[here, block] = v_act
                plain += v_act
                square += v_act * v_act
            index = lax.broadcasted_iota(jnp.int32, (chunk, LANES), 1)
            sum_out[here, :] = jnp.where(
                index == 0, jnp.sum(plain, axis=1, keepdims=True), jnp.sum(square, axis=1, keepdims=True)
            )

        save.wait()

    return pl.pallas_call(
        body,
        out_shape=[
            jax.ShapeDtypeStruct((count, width), BF),
            jax.ShapeDtypeStruct((count, tiles * LANES), F32),
            jax.ShapeDtypeStruct((count, tiles * LANES), F32),
            jax.ShapeDtypeStruct((count, LANES), F32),
        ],
        in_specs=[SMEM, SMEM] + [HBM] * 3 + [VMEM] * 3 + [HBM] * N_PIECES,
        out_specs=[HBM] + [VMEM] * 3,
        scratch_shapes=[
            pltpu.VMEM((blocks, columns, 2 * tiles * LANES), BF),
            pltpu.VMEM((count, width), BF),
            pltpu.SemaphoreType.DMA((n_copies + 4,)),
        ]
        + [pltpu.VMEM((count, width), BF)] * 3,
        compiler_params=params(),
        cost_estimate=cost(4 * count * width * tiles * LANES, 4 * width * tiles * LANES),
    )(
        ids,
        config["place"],
        *state,
        gain.reshape(blocks, columns),
        scales[0].reshape(tiles, LANES),
        scales[1].reshape(tiles, LANES),
        *pieces,
    )


def mixer_out(config, u_act, v_act, sums, other, layer, spatial_weight, spatial_bias, stage, pieces):
    blocks, tiles, chunk, width = config["blocks"], config["tiles"], config["chunk"], config["width"]
    count, channels = u_act.shape
    columns = width // blocks
    span = spatial_weight.shape[1]
    n_copies = len(stage.runs())
    share = 0.5 / channels

    def body(*refs):
        place, u_ref, v_ref, s_ref, o_ref, gain_ref, bias_ref, w_ref, b_ref = refs[:9]
        parts, refs = refs[9 : 9 + N_PIECES], refs[9 + N_PIECES :]
        out, w_out, mixed, sems = refs
        copies = fetches(stage, parts, w_out, sems, 0)
        for copy in copies:
            copy.start()
        total = s_ref[...] + o_ref[...]
        mean = total[:, 0:1] * share
        var = total[:, 1:2] * share - mean * mean
        factor = lax.rsqrt(var + EPS)
        keep = lax.broadcasted_iota(jnp.int32, (span, span), 0) >= lax.broadcasted_iota(jnp.int32, (span, span), 1)
        for t in range(tiles):
            n = place[t]
            block = slice(t * LANES, (t + 1) * LANES)
            v_normed = ((v_ref[:, block] - mean) * factor * gain_ref[pl.ds(n, 1), :] + bias_ref[pl.ds(n, 1), :]).astype(BF)
            side = jnp.concatenate([v_normed[m * span : (m + 1) * span] for m in range(count // span)], axis=1)
            w = jnp.where(keep, w_ref[n].astype(F32), 0.0).astype(BF)
            turned = jnp.dot(w, side, preferred_element_type=F32)
            shift = b_ref[n]
            for m in range(count // span):
                here = slice(m * span, (m + 1) * span)
                spatial = turned[:, m * LANES : (m + 1) * LANES] + shift
                mixed[here, block] = (u_ref[here, block] * spatial).astype(BF)
        for copy in copies:
            copy.wait()

        @pl.loop(0, count // chunk)
        def _(i):
            here = pl.ds(pl.multiple_of(i * chunk, chunk), chunk)
            left = mixed[here, :]
            for l in range(blocks):
                acc = jnp.dot(left, w_out[l, SPARE:, :], preferred_element_type=F32)
                terms = w_out[l, :SPARE, :].astype(F32)
                out[here, l * columns : (l + 1) * columns] = (acc * (terms[0:1] + terms[1:2] + terms[2:3])).astype(BF)

    return pl.pallas_call(
        body,
        out_shape=jax.ShapeDtypeStruct((count, width), BF),
        in_specs=[SMEM] + [VMEM] * 8 + [HBM] * N_PIECES,
        out_specs=VMEM,
        scratch_shapes=[
            pltpu.VMEM((blocks, SPARE + channels, columns), BF),
            pltpu.VMEM((count, channels), BF),
            pltpu.SemaphoreType.DMA((n_copies,)),
        ],
        compiler_params=params(),
        cost_estimate=cost(2 * count * width * channels, 2 * width * channels),
    )(
        config["place"],
        u_act,
        v_act,
        sums,
        other,
        layer[0].reshape(tiles, LANES),
        layer[1].reshape(tiles, LANES),
        spatial_weight,
        jnp.broadcast_to(spatial_bias[:, :, None], (tiles, span, LANES)),
        *pieces,
    )


SWAP = [(0, 1), (1, 0)]
NZ, NY = 4, 2


def join(body, shapes, flag, *values):
    return pl.pallas_call(
        body,
        out_shape=[jax.ShapeDtypeStruct(shape, BF) for shape in shapes],
        in_specs=[SMEM] + [VMEM] * len(values),
        out_specs=[VMEM] * len(shapes),
        compiler_params=params(),
        cost_estimate=cost(1000000, 4 * sum(v.size for v in values)),
    )(flag, *values)


def gather(stage, near, far, outer):
    at = lambda z, y: z * NY + y
    pairs = lambda hops: [(at(a, y), at(b, y)) for a, b in hops for y in range(NY)]
    across = [(at(z, y), at(z, 1 - y)) for z in range(NZ) for y in range(NY)]
    axis = stage.axis
    unit, head = stage.unit, stage.head
    all_z, all_y = head + len(stage.near) * unit, head + len(stage.near_y) * unit
    fz, fy = stage.fz * unit, stage.fy * unit

    def shape(blocks, size):
        out = [blocks, near.shape[1], near.shape[2]]
        out[axis] = size
        return tuple(out)

    def part(ref, block, start, size):
        return ref.at[block, pl.ds(start, size), :] if axis == 1 else ref.at[block, :, pl.ds(start, size)]

    def put(to, block, start, source, at, begin, size):
        part(to, block, start, size)[...] = part(source, at, begin, size)[...]

    def join_e(_, near_ref, e_ref, m_ref, y_ref):
        for k, ref in enumerate((near_ref, e_ref)):
            put(m_ref, k, 0, ref, 0, 0, all_z)
            put(y_ref, k, 0, ref, 0, 0, all_y)

    def join_p(_, e_ref, y_ref, p_ref):
        put(p_ref, 0, 0, e_ref, 0, head, fz)
        for k in range(2):
            put(p_ref, 0, fz + k * fy, y_ref, k, head, fy)

    def join_g(is_outer, g_ref, m_ref, two_ref, r_ref):
        def take(ref):
            for k in range(2):
                put(two_ref, k, 0, ref, k, 0, all_z)
                put(r_ref, k, 0, ref, k, 0, all_y)

        pl.when(is_outer[0] == 1)(lambda: take(g_ref))
        pl.when(is_outer[0] == 0)(lambda: take(m_ref))

    def join_q(_, two_ref, r_ref, q_ref):
        for k in range(2):
            put(q_ref, k, 0, two_ref, k, head, fz)
            put(q_ref, k, fz, r_ref, k, head, fy)

    e = lax.ppermute(near, "fs", pairs([(0, 1), (1, 0), (2, 3), (3, 2)]))
    m, y = join(join_e, [shape(2, all_z), shape(2, all_y)], outer, near, e)
    m = lax.ppermute(m, "fs", pairs([(1, 2), (2, 1)]))
    y = lax.ppermute(y, "fs", across)
    g = lax.ppermute(m, "fs", pairs([(1, 0), (2, 3)]))
    (p,) = join(join_p, [shape(1, fz + 2 * fy)], outer, e, y)
    p = lax.ppermute(p, "rep", SWAP)
    two, r = join(join_g, [shape(2, all_z), shape(2, all_y)], outer, g, m)
    r = lax.ppermute(r, "fs", across)
    (q,) = join(join_q, [shape(2, fz + fy)], outer, two, r)
    q = lax.ppermute(q, "rep", SWAP)
    return [near, e, two, far, y, r, p, q]


def fast(*args):
    (tokens, norm_first, norm_mix, norm_second, gate_weight, up_weight, down_weight, gate_scale, up_scale, down_scale,
     u_weight, v_weight, u_scale, v_scale, ln_gain, ln_bias, spatial_weight, spatial_bias, out_weight, out_scale) = args
    count, half = tokens.shape
    width = 2 * half
    blocks = NZ * NY
    columns = width // blocks
    rep, tp, fs = lax.axis_index("rep"), lax.axis_index("tp"), lax.axis_index("fs")
    z, y = fs // NY, fs % NY
    outer = jnp.logical_or(z == 0, z == NZ - 1).astype(jnp.int32).reshape(1)
    low = z < 2
    layers = (z, z + 1 - 2 * (z % 2), jnp.where(low, 2, 1), jnp.where(low, 3, 0))
    ids = jnp.stack([layer * NY + row for row in (y, 1 - y) for layer in layers] + [tp]).astype(jnp.int32)
    ff_tiles, bw_tiles = gate_weight.shape[1] // LANES, u_weight.shape[1] // LANES

    def places(tiles):
        index = jnp.arange(tiles, dtype=jnp.int32)
        return jnp.where(rep == 0, index, tiles - 1 - index)

    ff_place, bw_place = places(ff_tiles), places(bw_tiles)
    rim = ff_tiles // 5
    every = list(range(ff_tiles))
    outside = every[:rim] + [ff_tiles // 2] * (ff_tiles % 2) + every[ff_tiles - rim :]
    inside = [k for k in every if k not in outside]
    g1, g2 = Stage("g1", outside, 2 * LANES, 2, 0), Stage("g2", inside, 2 * LANES, 2, 0)
    dn = Stage("dn", every, LANES, 1, SPARE)
    uv = Stage("uv", list(range(bw_tiles)), 2 * LANES, 2, 0)
    ou = Stage("ou", list(range(bw_tiles)), LANES, 1, SPARE)
    own = {}
    own["g1"], own["g2"] = pack_pairs(gate_weight, up_weight, ff_place, [g1, g2])
    own["dn"] = pack_rows(down_weight, down_scale, ff_place, dn)
    (own["uv"],) = pack_pairs(u_weight, v_weight, bw_place, [uv])
    own["ou"] = pack_rows(out_weight, out_scale, bw_place, ou)
    peer = lax.ppermute(tokens, "tp", SWAP)
    pieces = {s.name: gather(s, *own[s.name], outer) for s in (g1, g2, dn, uv, ou)}
    full = jnp.where(tp == 0, jnp.concatenate([tokens, peer], axis=1), jnp.concatenate([peer, tokens], axis=1))
    start = jnp.concatenate([lax.dynamic_slice_in_dim(full, ids[l] * columns, columns, axis=1) for l in range(blocks)], axis=1)
    chunk = count // 2
    ff = {"blocks": blocks, "tiles": ff_tiles, "chunk": chunk, "place": ff_place, "width": width}
    mix = {"blocks": blocks, "tiles": bw_tiles, "chunk": chunk, "place": bw_place, "width": width}
    ff_stages, ff_pieces = (g1, g2, dn), [pieces["g1"], pieces["g2"], pieces["dn"]]
    hidden = first_hidden(ff, ids, start, norm_first, ff_stages[:2], ff_pieces[:2], (gate_scale, up_scale))
    first = first_down(ff, hidden, dn, pieces["dn"])
    first_in = lax.ppermute(first, "tp", SWAP)
    middle, u_act, v_act, sums = mixer_in(mix, ids, (start, first, first_in), norm_mix, uv, pieces["uv"], (u_scale, v_scale))
    sums_in = lax.ppermute(sums, "tp", SWAP)
    mixed = mixer_out(mix, u_act, v_act, sums, sums_in, (ln_gain, ln_bias), spatial_weight, spatial_bias, ou, pieces["ou"])
    mixed_in = lax.ppermute(mixed, "tp", SWAP)
    own_last, send, rest = feed_forward(
        ff, ids, (middle, mixed, mixed_in), norm_second, ff_stages, ff_pieces, (gate_scale, up_scale), True)
    got = lax.ppermute(send, "tp", SWAP)
    return (rest.astype(F32) + 0.5 * (own_last.astype(F32) + got.astype(F32))).astype(BF)


def plain(*args):
    (tokens, norm_first, norm_mix, norm_second, gate_weight, up_weight, down_weight, gate_scale, up_scale, down_scale,
     u_weight, v_weight, u_scale, v_scale, ln_gain, ln_bias, spatial_weight, spatial_bias, out_weight, out_scale) = args
    gather = lambda v, axis: lax.all_gather(v, "fs", axis=axis, tiled=True)
    count, n_tp = tokens.shape[0], lax.axis_size("tp")
    span = spatial_weight.shape[1]

    def full_norm(rows, gain):
        values = lax.all_gather(rows, "tp", axis=1, tiled=True).astype(F32)
        factor = lax.rsqrt(jnp.mean(values * values, axis=1, keepdims=True) + EPS)
        return (values * factor * gain).astype(BF)

    def spread_sum(term):
        return lax.psum_scatter(term.astype(BF), "tp", scatter_dimension=1, tiled=True).astype(F32)

    def dot(left, right):
        return jnp.dot(left, right, preferred_element_type=F32)

    gate_all, up_all, down_all = gather(gate_weight.astype(BF), 0), gather(up_weight.astype(BF), 0), gather(down_weight.astype(BF), 1)
    down_scales, out_scales = gather(down_scale, 0), gather(out_scale, 0)

    def feed(rows, gain):
        normed = full_norm(rows, gain)
        hidden = (jax.nn.silu(dot(normed, gate_all) * gate_scale) * (dot(normed, up_all) * up_scale)).astype(BF)
        return spread_sum(dot(hidden, down_all) * down_scales)

    middle = (tokens.astype(F32) + 0.5 * feed(tokens, norm_first)).astype(BF)
    normed = full_norm(middle, norm_mix)
    u_pre = dot(normed, gather(u_weight.astype(BF), 0)) * u_scale
    v_act = gelu(dot(normed, gather(v_weight.astype(BF), 0)) * v_scale)
    sums = lax.psum((jnp.sum(v_act, axis=1), jnp.sum(v_act * v_act, axis=1)), "tp")
    channels = v_act.shape[1]
    v_mean = (sums[0] / (n_tp * channels))[:, None]
    v_var = (sums[1] / (n_tp * channels))[:, None] - v_mean * v_mean
    v_normed = ((v_act - v_mean) * lax.rsqrt(v_var + EPS) * ln_gain + ln_bias).astype(BF)
    groups = spatial_weight.shape[0]
    tiles = v_normed.reshape(count // span, span, groups, channels // groups)
    lower = jnp.tril(jnp.ones((span, span), jnp.bool_))
    masked = jnp.where(lower[None], spatial_weight, jnp.zeros_like(spatial_weight))
    spatial = jnp.einsum("gts,nsgc->ntgc", masked, tiles, preferred_element_type=F32) + spatial_bias.T[None, :, :, None]
    mixed = (gelu(u_pre) * spatial.reshape(count, channels)).astype(BF)
    second = (middle.astype(F32) + spread_sum(dot(mixed, gather(out_weight.astype(BF), 1)) * out_scales)).astype(BF)
    return (second.astype(F32) + 0.5 * feed(second, norm_second)).astype(BF)


def solution(mesh):
    tokens = P(("rep", "fs"), "tp")
    rows, columns = P("fs", "tp"), P("tp", "fs")
    tp, fs, whole = P("tp"), P("fs"), P()
    placed = (
        tokens, whole, whole, whole, rows, rows, columns, tp, tp, fs, rows, rows, tp, tp, tp, tp,
        P("tp", None, None), P("tp", None), columns, fs,
    )

    def on_device(*args):
        block = args[4].shape[0]
        tidy = block % (2 * LANES) == 0 and args[4].shape[1] % LANES == 0 and args[10].shape[1] % LANES == 0
        if tidy and mesh.shape["fs"] == NZ * NY and mesh.shape["rep"] == 2 and mesh.shape["tp"] == 2:
            return fast(*args)
        return plain(*args)

    return jax.shard_map(on_device, mesh=mesh, in_specs=placed, out_specs=tokens, check_vma=False)
```

profile of v0, /device:TPU:0, one launch (start us, length us, event | category | flops | bytes accessed | tf_op | source)
XLA Modules:
  0.0 431.4 jit_solution(4877958093740014398)
XLA Ops:
  0.5 3.2 shard_map.190
  6.7 14.9 %collective-permute-done.8.e_ref.refs_9_.refs_17_ = bf16[1,256,1280]{2,1,0:T(8,128)(2,1)S(1)} collective-permute-done((bf16[1,256,1280]{2,1,0:T(8,128)(2,1)}, bf16[1,256,1280]{2,1,0:T(8,128)(2,1)S(1)}, u32[]{:S(2)}, u32[]{:S(2)}) %collective-permute-start.8) | collective-permute-done | bytes 655392 | tf_op jit(solution)/shard_map/ppermute | solution.py:584
  28.3 4.5 %collective-permute-start.15 = (bf16[1,1168,256]{2,1,0:T(8,128)(2,1)}, bf16[1,1168,256]{2,1,0:T(8,128)(2,1)S(1)}, u32[]{:S(2)}, u32[]{:S(2)}) collective-permute-start(bf16[1,1168,256]{2,1,0:T(8,128)(2,1)} %get-tuple-element.54.near_ref.refs_0_.refs_24_), channel_id=1, source_target_pairs={{0,4},{2,6},{4,0},{6,2},{8,12},{10,14},{12,8},{14,10},{1,5},{3,7},... | collective-permute-start | bytes 1794056 | tf_op jit(solution)/shard_map/ppermute | solution.py:584
  32.9 14.5 %collective-permute-done.15.e_ref.refs_1_.refs_25_ = bf16[1,1168,256]{2,1,0:T(8,128)(2,1)S(1)} collective-permute-done((bf16[1,1168,256]{2,1,0:T(8,128)(2,1)}, bf16[1,1168,256]{2,1,0:T(8,128)(2,1)S(1)}, u32[]{:S(2)}, u32[]{:S(2)}) %collective-permute-start.15) | collective-permute-done | bytes 598048 | tf_op jit(solution)/shard_map/ppermute | solution.py:584
  52.6 4.0 collective-permute-done.1.e_ref.refs_1_.refs_9_
  68.4 43.5 %collective-permute-start.23 = (bf16[1,256,768]{2,1,0:T(8,128)(2,1)}, bf16[1,256,768]{2,1,0:T(8,128)(2,1)S(1)}, u32[]{:S(2)}, u32[]{:S(2)}) collective-permute-start(bf16[1,256,768]{2,1,0:T(8,128)(2,1)} %get-tuple-element.60.near_ref.refs_8_), channel_id=1, source_target_pairs={{0,4},{2,6},{4,0},{6,2},{8,12},{10,14},{12,8},{14,10},{1,5},{3,7},... | collective-permute-start | bytes 1179656 | tf_op jit(solution)/shard_map/ppermute | solution.py:584
  113.0 3.2 shard_map.196
  117.7 31.2 %collective-permute-done.23.e_ref.refs_9_ = bf16[1,256,768]{2,1,0:T(8,128)(2,1)S(1)} collective-permute-done((bf16[1,256,768]{2,1,0:T(8,128)(2,1)}, bf16[1,256,768]{2,1,0:T(8,128)(2,1)S(1)}, u32[]{:S(2)}, u32[]{:S(2)}) %collective-permute-start.23) | collective-permute-done | bytes 393248 | tf_op jit(solution)/shard_map/ppermute | solution.py:584
  176.8 9.7 %collective-permute-done.11.y_ref.refs_12_.refs_20_ = bf16[2,256,768]{2,1,0:T(8,128)(2,1)} collective-permute-done((bf16[2,256,768]{2,1,0:T(8,128)(2,1)}, bf16[2,256,768]{2,1,0:T(8,128)(2,1)}, u32[]{:S(2)}, u32[]{:S(2)}) %collective-permute-start.11) | collective-permute-done | bytes 786464 | tf_op jit(solution)/shard_map/ppermute | solution.py:587
  191.1 29.4 %collective-permute-done.5.r_ref.refs_5_.refs_13_ = bf16[2,256,768]{2,1,0:T(8,128)(2,1)} collective-permute-done((bf16[2,256,768]{2,1,0:T(8,128)(2,1)}, bf16[2,256,768]{2,1,0:T(8,128)(2,1)}, u32[]{:S(2)}, u32[]{:S(2)}) %collective-permute-start.5) | collective-permute-done | bytes 786464 | tf_op jit(solution)/shard_map/ppermute | solution.py:592
  241.2 13.9 %collective-permute-done.7.refs_7_.refs_15_ = bf16[2,256,768]{2,1,0:T(8,128)(2,1)} collective-permute-done((bf16[2,256,768]{2,1,0:T(8,128)(2,1)}, bf16[2,256,768]{2,1,0:T(8,128)(2,1)}, u32[]{:S(2)}, u32[]{:S(2)}) %collective-permute-start.7) | collective-permute-done | bytes 786464 | tf_op jit(solution)/shard_map/ppermute | solution.py:594
  255.1 15.4 %shard_map.199.left_ref = bf16[640,1408]{1,0:T(8,128)(2,1)} custom-call(s32[9]{0:T(128)} %stack.39.at.refs_0_, s32[11]{0:T(128)} %broadcast_select_fusion.1.at.place.refs_1_, bf16[640,2048]{1,0:T(8,128)(2,1)} %dynamic-slice_dynamic-update-slice_fusion.source.refs_2_, f32[8,256]{1,0:T(8,128)} %reshape.41.gain_ref, f32[11,128]{1,0:T(8,128)} %bitcast.24, ...), custom_call_target="tpu_custom_call" | custom-call | flops 7381975040 | bytes 11534336 | tf_op jit(solution)/shard_map/pallas_call | solution.py:317
  270.5 12.9 %collective-permute-done.20.refs_6_.refs_30_ = bf16[1,1536,256]{2,1,0:T(8,128)(2,1)} collective-permute-done((bf16[1,1536,256]{2,1,0:T(8,128)(2,1)}, bf16[1,1536,256]{2,1,0:T(8,128)(2,1)}, u32[]{:S(2)}, u32[]{:S(2)}) %collective-permute-start.20) | collective-permute-done | bytes 786464 | tf_op jit(solution)/shard_map/ppermute | solution.py:590
  283.4 10.2 %shard_map.205.refs_3_ = bf16[640,2048]{1,0:T(8,128)(2,1)} custom-call(bf16[640,1408]{1,0:T(8,128)(2,1)} %shard_map.199.left_ref, bf16[1,1168,256]{2,1,0:T(8,128)(2,1)} %get-tuple-element.54.near_ref.refs_0_.refs_24_, bf16[1,1168,256]{2,1,0:T(8,128)(2,1)} %copy-done.3, bf16[2,1168,256]{2,1,0:T(8,128)(2,1)} %get-tuple-element.56.two_ref.refs_2_.refs_26_, ...), custom_call_target="tpu_custom_call" | custom-call | flops 3690987520 | bytes 5767168 | tf_op jit(solution)/shard_map/pallas_call | solution.py:364
  295.0 20.6 %collective-permute-done.25.g_ref = bf16[2,256,768]{2,1,0:T(8,128)(2,1)} collective-permute-done((bf16[2,256,768]{2,1,0:T(8,128)(2,1)S(1)}, bf16[2,256,768]{2,1,0:T(8,128)(2,1)}, u32[]{:S(2)}, u32[]{:S(2)}) %collective-permute-start.25) | collective-permute-done | bytes 786464 | tf_op jit(solution)/shard_map/ppermute | solution.py:588
  322.0 6.0 %collective-permute-done.31.e_ref.refs_10_ = bf16[1,400,256]{2,1,0:T(8,128)(2,1)S(1)} collective-permute-done((bf16[1,400,256]{2,1,0:T(8,128)(2,1)}, bf16[1,400,256]{2,1,0:T(8,128)(2,1)S(1)}, u32[]{:S(2)}, u32[]{:S(2)}) %collective-permute-start.31) | collective-permute-done | bytes 204832 | tf_op jit(solution)/shard_map/ppermute | solution.py:584
  339.0 4.1 collective-permute-done.26.y_ref.refs_12_
  349.0 3.1 collective-permute-done.33.g_ref
  365.9 5.1 %collective-permute-done.28.refs_14_ = bf16[1,256,1280]{2,1,0:T(8,128)(2,1)} collective-permute-done((bf16[1,256,1280]{2,1,0:T(8,128)(2,1)}, bf16[1,256,1280]{2,1,0:T(8,128)(2,1)}, u32[]{:S(2)}, u32[]{:S(2)}) %collective-permute-start.28) | collective-permute-done | bytes 655392 | tf_op jit(solution)/shard_map/ppermute | solution.py:590
  372.5 12.3 %shard_map.211 = (bf16[640,2048]{1,0:T(8,128)(2,1)}, f32[640,512]{1,0:T(8,128)}, f32[640,512]{1,0:T(8,128)}, f32[640,128]{1,0:T(8,128)}) custom-call(s32[9]{0:T(128)} %stack.39.at.refs_0_, s32[4]{0:T(128)} %broadcast_select_fusion.at.refs_1_.refs_0_, bf16[640,2048]{1,0:T(8,128)(2,1)} %dynamic-slice_dynamic-update-slice_fusion.source.refs_2_, ...), custom_call_target="tpu_custom_call" | custom-call | flops 2684354560 | bytes 4194304 | tf_op jit(solution)/shard_map/pallas_call | solution.py:426
  387.7 7.4 %shard_map.217.refs_3_ = bf16[640,2048]{1,0:T(8,128)(2,1)} custom-call(s32[4]{0:T(128)} %broadcast_select_fusion.at.refs_1_.refs_0_, f32[640,512]{1,0:T(8,128)} %get-tuple-element.67.refs_1_, f32[640,512]{1,0:T(8,128)} %get-tuple-element.68.refs_2_, f32[640,128]{1,0:T(8,128)} %get-tuple-element.69.refs_3_, f32[640,128]{1,0:T(8,128)} %copy-done.22, ...), custom_call_target="tpu_custom_call" | custom-call | flops 1342177280 | bytes 2097152 | tf_op jit(solution)/shard_map/pallas_call | solution.py:499
  395.9 4.4 %collective-permute-done.38.refs_4_ = bf16[640,2048]{1,0:T(8,128)(2,1)S(1)} collective-permute-done((bf16[640,2048]{1,0:T(8,128)(2,1)}, bf16[640,2048]{1,0:T(8,128)(2,1)S(1)}, u32[]{:S(2)}, u32[]{:S(2)}) %collective-permute-start.38) | collective-permute-done | bytes 2621472 | tf_op jit(solution)/shard_map/ppermute | solution.py:645
  401.8 22.6 %shard_map.218 = (bf16[640,1024]{1,0:T(8,128)(2,1)}, bf16[640,1024]{1,0:T(8,128)(2,1)}, bf16[640,1024]{1,0:T(8,128)(2,1)}) custom-call(s32[9]{0:T(128)} %stack.39.at.refs_0_, s32[11]{0:T(128)} %broadcast_select_fusion.1.at.place.refs_1_, bf16[640,2048]{1,0:T(8,128)(2,1)} %get-tuple-element.66.refs_2_, bf16[640,2048]{1,0:T(8,128)(2,1)} %shard_map.217.refs_3_, ...), custom_call_target="tpu_custom_call" | custom-call | flops 11072962560 | bytes 17301504 | tf_op jit(solution)/shard_map/pallas_call | solution.py:268
  427.7 3.6 add_convert_fusion
  (158 shorter events, 131.3 us)
Async XLA Ops:
  25.2 36.5 %collective-permute-start.9 = (bf16[2,256,1280]{2,1,0:T(8,128)(2,1)}, bf16[2,256,1280]{2,1,0:T(8,128)(2,1)S(1)}, u32[]{:S(2)}, u32[]{:S(2)}) collective-permute-start(bf16[2,256,1280]{2,1,0:T(8,128)(2,1)} %get-tuple-element.49), channel_id=1, source_target_pairs={{4,8},{6,10},{8,4},{10,6},{5,9},{7,11},{9,5},{11,7},{20,24},{22,26... | collective-permute-start | bytes 3932168 | tf_op jit(solution)/shard_map/ppermute | solution.py:586
  32.8 23.8 %collective-permute-start.1 = (bf16[1,256,1024]{2,1,0:T(8,128)(2,1)S(1)}, bf16[1,256,1024]{2,1,0:T(8,128)(2,1)S(1)}, u32[]{:S(2)}, u32[]{:S(2)}) collective-permute-start(bf16[1,256,1024]{2,1,0:T(8,128)(2,1)S(1)} %copy-done.17), channel_id=1, source_target_pairs={{0,4},{2,6},{4,0},{6,2},{8,12},{10,14},{12,8},{14,10},{1,5},{3,7},... | collective-permute-start | bytes 1572872 | tf_op jit(solution)/shard_map/ppermute | solution.py:584
  61.7 50.2 %collective-permute-start.10 = (bf16[2,256,1280]{2,1,0:T(8,128)(2,1)S(1)}, bf16[2,256,1280]{2,1,0:T(8,128)(2,1)S(1)}, u32[]{:S(2)}, u32[]{:S(2)}) collective-permute-start(bf16[2,256,1280]{2,1,0:T(8,128)(2,1)S(1)} %collective-permute-done.9.m_ref), channel_id=1, source_target_pairs={{4,0},{6,2},{8,12},{10,14},{5,1},{7,3},{9,13},{11,15},{20,16},{22,... | collective-permute-start | bytes 3932168 | tf_op jit(solution)/shard_map/ppermute | solution.py:588
  63.0 87.4 %collective-permute-start.17 = (bf16[2,1168,256]{2,1,0:T(8,128)(2,1)}, bf16[2,1168,256]{2,1,0:T(8,128)(2,1)}, u32[]{:S(2)}, u32[]{:S(2)}) collective-permute-start(bf16[2,1168,256]{2,1,0:T(8,128)(2,1)} %collective-permute-done.16.m_ref), channel_id=1, source_target_pairs={{4,0},{6,2},{8,12},{10,14},{5,1},{7,3},{9,13},{11,15},{20,16},{22,... | collective-permute-start | bytes 3588104 | tf_op jit(solution)/shard_map/ppermute | solution.py:588
  64.3 89.7 %collective-permute-start.3 = (bf16[2,256,1024]{2,1,0:T(8,128)(2,1)}, bf16[2,256,1024]{2,1,0:T(8,128)(2,1)}, u32[]{:S(2)}, u32[]{:S(2)}) collective-permute-start(bf16[2,256,1024]{2,1,0:T(8,128)(2,1)} %collective-permute-done.2.m_ref), channel_id=1, source_target_pairs={{4,0},{6,2},{8,12},{10,14},{5,1},{7,3},{9,13},{11,15},{20,16},{22,... | collective-permute-start | bytes 3145736 | tf_op jit(solution)/shard_map/ppermute | solution.py:588
  65.6 99.6 %collective-permute-start = (bf16[640,1024]{1,0:T(8,128)(2,1)}, bf16[640,1024]{1,0:T(8,128)(2,1)}, u32[]{:S(2)}, u32[]{:S(2)}) collective-permute-start(bf16[640,1024]{1,0:T(8,128)(2,1)} %param.20), channel_id=1, source_target_pairs={{0,1},{1,0},{2,3},{3,2},{4,5},{5,4},{6,7},{7,6},{8,9},{9,8},{10,11... | collective-permute-start | bytes 3932168 | tf_op jit(solution)/shard_map/ppermute | solution.py:631
  68.4 80.5 %collective-permute-start.23 = (bf16[1,256,768]{2,1,0:T(8,128)(2,1)}, bf16[1,256,768]{2,1,0:T(8,128)(2,1)S(1)}, u32[]{:S(2)}, u32[]{:S(2)}) collective-permute-start(bf16[1,256,768]{2,1,0:T(8,128)(2,1)} %get-tuple-element.60.near_ref.refs_8_), channel_id=1, source_target_pairs={{0,4},{2,6},{4,0},{6,2},{8,12},{10,14},{12,8},{14,10},{1,5},{3,7},... | collective-permute-start | bytes 1179656 | tf_op jit(solution)/shard_map/ppermute | solution.py:584
  116.2 42.4 %collective-permute-start.12 = (bf16[2,256,768]{2,1,0:T(8,128)(2,1)}, bf16[2,256,768]{2,1,0:T(8,128)(2,1)S(1)}, u32[]{:S(2)}, u32[]{:S(2)}) collective-permute-start(bf16[2,256,768]{2,1,0:T(8,128)(2,1)} %get-tuple-element.53), channel_id=1, source_target_pairs={{0,2},{2,0},{4,6},{6,4},{8,10},{10,8},{12,14},{14,12},{1,3},{3,1},... | collective-permute-start | bytes 2359304 | tf_op jit(solution)/shard_map/ppermute | solution.py:592
  150.4 36.1 %collective-permute-start.11 = (bf16[2,256,768]{2,1,0:T(8,128)(2,1)}, bf16[2,256,768]{2,1,0:T(8,128)(2,1)}, u32[]{:S(2)}, u32[]{:S(2)}) collective-permute-start(bf16[2,256,768]{2,1,0:T(8,128)(2,1)} %get-tuple-element.52), channel_id=1, source_target_pairs={{0,2},{2,0},{4,6},{6,4},{8,10},{10,8},{12,14},{14,12},{1,3},{3,1},... | collective-permute-start | bytes 2359304 | tf_op jit(solution)/shard_map/ppermute | solution.py:587
  154.0 70.4 %collective-permute-start.19 = (bf16[2,784,256]{2,1,0:T(8,128)(2,1)}, bf16[2,784,256]{2,1,0:T(8,128)(2,1)}, u32[]{:S(2)}, u32[]{:S(2)}) collective-permute-start(bf16[2,784,256]{2,1,0:T(8,128)(2,1)} %get-tuple-element.59), channel_id=1, source_target_pairs={{0,2},{2,0},{4,6},{6,4},{8,10},{10,8},{12,14},{14,12},{1,3},{3,1},... | collective-permute-start | bytes 2408456 | tf_op jit(solution)/shard_map/ppermute | solution.py:592
  158.6 62.0 %collective-permute-start.5 = (bf16[2,256,768]{2,1,0:T(8,128)(2,1)}, bf16[2,256,768]{2,1,0:T(8,128)(2,1)}, u32[]{:S(2)}, u32[]{:S(2)}) collective-permute-start(bf16[2,256,768]{2,1,0:T(8,128)(2,1)} %get-tuple-element.47), channel_id=1, source_target_pairs={{0,2},{2,0},{4,6},{6,4},{8,10},{10,8},{12,14},{14,12},{1,3},{3,1},... | collective-permute-start | bytes 2359304 | tf_op jit(solution)/shard_map/ppermute | solution.py:592
  165.2 68.9 %collective-permute-start.18 = (bf16[2,784,256]{2,1,0:T(8,128)(2,1)}, bf16[2,784,256]{2,1,0:T(8,128)(2,1)}, u32[]{:S(2)}, u32[]{:S(2)}) collective-permute-start(bf16[2,784,256]{2,1,0:T(8,128)(2,1)} %get-tuple-element.58), channel_id=1, source_target_pairs={{0,2},{2,0},{4,6},{6,4},{8,10},{10,8},{12,14},{14,12},{1,3},{3,1},... | collective-permute-start | bytes 2408456 | tf_op jit(solution)/shard_map/ppermute | solution.py:587
  170.4 84.7 %collective-permute-start.14 = (bf16[2,256,1024]{2,1,0:T(8,128)(2,1)}, bf16[2,256,1024]{2,1,0:T(8,128)(2,1)}, u32[]{:S(2)}, u32[]{:S(2)}) collective-permute-start(bf16[2,256,1024]{2,1,0:T(8,128)(2,1)} %shard_map.198), channel_id=1, source_target_pairs={{0,16},{16,0},{1,17},{17,1},{2,18},{18,2},{3,19},{19,3},{4,20},{20... | collective-permute-start | bytes 3145736 | tf_op jit(solution)/shard_map/ppermute | solution.py:594
  188.8 51.6 %collective-permute-start.13 = (bf16[1,256,1792]{2,1,0:T(8,128)(2,1)}, bf16[1,256,1792]{2,1,0:T(8,128)(2,1)}, u32[]{:S(2)}, u32[]{:S(2)}) collective-permute-start(bf16[1,256,1792]{2,1,0:T(8,128)(2,1)} %shard_map.197), channel_id=1, source_target_pairs={{0,16},{16,0},{1,17},{17,1},{2,18},{18,2},{3,19},{19,3},{4,20},{20... | collective-permute-start | bytes 2752520 | tf_op jit(solution)/shard_map/ppermute | solution.py:590
  224.5 30.7 %collective-permute-start.7 = (bf16[2,256,768]{2,1,0:T(8,128)(2,1)}, bf16[2,256,768]{2,1,0:T(8,128)(2,1)}, u32[]{:S(2)}, u32[]{:S(2)}) collective-permute-start(bf16[2,256,768]{2,1,0:T(8,128)(2,1)} %shard_map.194), channel_id=1, source_target_pairs={{0,16},{16,0},{1,17},{17,1},{2,18},{18,2},{3,19},{19,3},{4,20},{20... | collective-permute-start | bytes 2359304 | tf_op jit(solution)/shard_map/ppermute | solution.py:594
  234.1 49.3 %collective-permute-start.21 = (bf16[2,896,256]{2,1,0:T(8,128)(2,1)}, bf16[2,896,256]{2,1,0:T(8,128)(2,1)}, u32[]{:S(2)}, u32[]{:S(2)}) collective-permute-start(bf16[2,896,256]{2,1,0:T(8,128)(2,1)} %shard_map.204), channel_id=1, source_target_pairs={{0,16},{16,0},{1,17},{17,1},{2,18},{18,2},{3,19},{19,3},{4,20},{20... | collective-permute-start | bytes 2752520 | tf_op jit(solution)/shard_map/ppermute | solution.py:594
  238.6 44.8 %collective-permute-start.20 = (bf16[1,1536,256]{2,1,0:T(8,128)(2,1)}, bf16[1,1536,256]{2,1,0:T(8,128)(2,1)}, u32[]{:S(2)}, u32[]{:S(2)}) collective-permute-start(bf16[1,1536,256]{2,1,0:T(8,128)(2,1)} %shard_map.203), channel_id=1, source_target_pairs={{0,16},{16,0},{1,17},{17,1},{2,18},{18,2},{3,19},{19,3},{4,20},{20... | collective-permute-start | bytes 2359304 | tf_op jit(solution)/shard_map/ppermute | solution.py:590
  240.5 53.2 %collective-permute-start.24 = (bf16[2,256,768]{2,1,0:T(8,128)(2,1)}, bf16[2,256,768]{2,1,0:T(8,128)(2,1)S(1)}, u32[]{:S(2)}, u32[]{:S(2)}) collective-permute-start(bf16[2,256,768]{2,1,0:T(8,128)(2,1)} %get-tuple-element.61), channel_id=1, source_target_pairs={{4,8},{6,10},{8,4},{10,6},{5,9},{7,11},{9,5},{11,7},{20,24},{22,26... | collective-permute-start | bytes 2359304 | tf_op jit(solution)/shard_map/ppermute | solution.py:586
  293.6 77.4 %collective-permute-start.22 = (bf16[640,2048]{1,0:T(8,128)(2,1)}, bf16[640,2048]{1,0:T(8,128)(2,1)S(1)}, u32[]{:S(2)}, u32[]{:S(2)}) collective-permute-start(bf16[640,2048]{1,0:T(8,128)(2,1)} %shard_map.205.refs_3_), channel_id=1, source_target_pairs={{0,1},{1,0},{2,3},{3,2},{4,5},{5,4},{6,7},{7,6},{8,9},{9,8},{10,11... | collective-permute-start | bytes 7864328 | tf_op jit(solution)/shard_map/ppermute | solution.py:641
  293.7 21.9 %collective-permute-start.25 = (bf16[2,256,768]{2,1,0:T(8,128)(2,1)S(1)}, bf16[2,256,768]{2,1,0:T(8,128)(2,1)}, u32[]{:S(2)}, u32[]{:S(2)}) collective-permute-start(bf16[2,256,768]{2,1,0:T(8,128)(2,1)S(1)} %collective-permute-done.24.m_ref), channel_id=1, source_target_pairs={{4,0},{6,2},{8,12},{10,14},{5,1},{7,3},{9,13},{11,15},{20,16},{22,... | collective-permute-start | bytes 2359304 | tf_op jit(solution)/shard_map/ppermute | solution.py:588
  321.5 21.6 %collective-permute-start.26 = (bf16[2,256,512]{2,1,0:T(8,128)(2,1)}, bf16[2,256,512]{2,1,0:T(8,128)(2,1)S(1)}, u32[]{:S(2)}, u32[]{:S(2)}) collective-permute-start(bf16[2,256,512]{2,1,0:T(8,128)(2,1)} %get-tuple-element.64), channel_id=1, source_target_pairs={{0,2},{2,0},{4,6},{6,4},{8,10},{10,8},{12,14},{14,12},{1,3},{3,1},... | collective-permute-start | bytes 1572872 | tf_op jit(solution)/shard_map/ppermute | solution.py:587
  336.2 34.8 %collective-permute-start.29 = (bf16[2,256,768]{2,1,0:T(8,128)(2,1)}, bf16[2,256,768]{2,1,0:T(8,128)(2,1)}, u32[]{:S(2)}, u32[]{:S(2)}) collective-permute-start(bf16[2,256,768]{2,1,0:T(8,128)(2,1)} %shard_map.210), channel_id=1, source_target_pairs={{0,16},{16,0},{1,17},{17,1},{2,18},{18,2},{3,19},{19,3},{4,20},{20... | collective-permute-start | bytes 2359304 | tf_op jit(solution)/shard_map/ppermute | solution.py:594
  345.9 25.0 %collective-permute-start.28 = (bf16[1,256,1280]{2,1,0:T(8,128)(2,1)}, bf16[1,256,1280]{2,1,0:T(8,128)(2,1)}, u32[]{:S(2)}, u32[]{:S(2)}) collective-permute-start(bf16[1,256,1280]{2,1,0:T(8,128)(2,1)} %shard_map.209), channel_id=1, source_target_pairs={{0,16},{16,0},{1,17},{17,1},{2,18},{18,2},{3,19},{19,3},{4,20},{20... | collective-permute-start | bytes 1966088 | tf_op jit(solution)/shard_map/ppermute | solution.py:590
  359.4 25.6 %collective-permute-start.36 = (bf16[1,640,256]{2,1,0:T(8,128)(2,1)}, bf16[1,640,256]{2,1,0:T(8,128)(2,1)S(1)}, u32[]{:S(2)}, u32[]{:S(2)}) collective-permute-start(bf16[1,640,256]{2,1,0:T(8,128)(2,1)} %shard_map.215), channel_id=1, source_target_pairs={{0,16},{16,0},{1,17},{17,1},{2,18},{18,2},{3,19},{19,3},{4,20},{20... | collective-permute-start | bytes 983048 | tf_op jit(solution)/shard_map/ppermute | solution.py:590
  (44 other events, 459.7 us)
where the time goes:
time: 433 us; the launch traced here: 431 us
  waiting for transfers between devices  187 us (43%)
  Pallas kernels  126 us (29%)
  starting transfers between devices  88.3 us (20%)
  local copies, waits for them, and re-layouts  22.5 us (5%)
  other arithmetic  7.44 us (2%)
    ppermute x5, waiting for transfers between devices, gather(): e = lax.ppermute(near, 'fs', pairs([(0, 1), (1, 0), (2, 3), (3, 2)]))  70.7 us
    ppermute x5, starting transfers between devices, gather(): e = lax.ppermute(near, 'fs', pairs([(0, 1), (1, 0), (2, 3), (3, 2)]))  51.1 us
    pallas_call x20, Pallas kernels, join(): pl.pallas_call(body, out_shape=[jax.ShapeDtypeStruct(shape, BF) for shape...  48.6 us
    ppermute x5, waiting for transfers between devices, gather(): r = lax.ppermute(r, 'fs', across)  32.2 us
    ppermute x5, waiting for transfers between devices, gather(): g = lax.ppermute(m, 'fs', pairs([(1, 0), (2, 3)]))  23.7 us
    pallas_call x1, Pallas kernels, feed_forward(): pl.pallas_call(body, out_shape=shapes, in_specs=[SMEM, SMEM] + [HBM] * n_...  22.6 us
    ppermute x5, waiting for transfers between devices, gather(): y = lax.ppermute(y, 'fs', across)  19 us
    ppermute x5, waiting for transfers between devices, gather(): p = lax.ppermute(p, 'rep', SWAP)  18 us
  transfers between devices with their start and end apart: 40, of which 20 were waited for; matrix products, arithmetic and copies ran while one was open for 3% of the time, Pallas kernels for 21%

commit v1 on v0

--- a/solution.py
+++ b/solution.py
@@ -10,13 +10,14 @@
 LANES = 128
 SPARE = 16
 HBM = pl.BlockSpec(memory_space=pltpu.HBM)
+ANY = pl.BlockSpec(memory_space=pl.ANY)
 VMEM = pl.BlockSpec(memory_space=pltpu.VMEM)
 SMEM = pl.BlockSpec(memory_space=pltpu.SMEM)
 BF, F32 = jnp.bfloat16, jnp.float32
 
 
-def params():
-    return pltpu.CompilerParams(vmem_limit_bytes=60 * 1024 * 1024)
+def params(mebibytes):
+    return pltpu.CompilerParams(vmem_limit_bytes=mebibytes * 1024 * 1024)
 
 
 def cost(flops, size):
@@ -48,7 +49,7 @@
         out_shape=shapes,
         in_specs=[SMEM, VMEM, VMEM],
         out_specs=[VMEM] * len(shapes),
-        compiler_params=params(),
+        compiler_params=params(16),
         cost_estimate=cost(1000, 6 * left.size * 2),
     )(places, left, right)
     return [(out[2 * i], out[2 * i + 1]) for i in range(len(stages))]
@@ -79,7 +80,7 @@
         ],
         in_specs=[SMEM, VMEM, VMEM],
         out_specs=[VMEM, VMEM],
-        compiler_params=params(),
+        compiler_params=params(16),
         cost_estimate=cost(1000, 6 * weight.size),
     )(places, weight, scale.reshape(1, columns))
 
@@ -155,12 +156,12 @@
     return jnp.concatenate([gain_ref[pl.ds(at[l], 1), :] for l in range(blocks)], axis=1)
 
 
-def residual_and_norm(rest, weight, terms, gains, new_ref, normed, step):
-    count, _ = rest.shape
+def residual_and_norm(rest, weight, terms, gains, new_ref, normed, step, first=0, count=None):
+    count = rest.shape[0] if count is None else count
 
     @pl.loop(0, count // step, unroll=4)
     def _(i):
-        here = pl.ds(pl.multiple_of(i * step, step), step)
+        here = pl.ds(pl.multiple_of(first + i * step, step), step)
         rows = rest[here, :]
         if terms:
             total = terms[0][here, :].astype(F32) + terms[1][here, :].astype(F32)
@@ -169,9 +170,27 @@
         normed[here, :] = norm_rows(rows, gains)
 
 
+def norm_block(rest, weight, terms, gains, new_ref, normed, row, step):
+    here = slice(row, row + step)
+    rows = rest[here, :]
+    total = terms[0][here, :].astype(F32) + terms[1][here, :].astype(F32)
+    rows = (rows.astype(F32) + weight * total).astype(BF)
+    new_ref[here, :] = rows
+    normed[here, :] = norm_rows(rows, gains)
+
+
 def flat(ref, columns):
     block = ref[:, :, columns]
     return block.reshape(block.shape[0] * block.shape[1], block.shape[2])
+
+
+def hidden_tile(k, place, lhs, w_up, gs_ref, us_ref, out, here):
+    rhs = flat(w_up, slice(2 * k * LANES, (2 * k + 2) * LANES))
+    acc = jnp.dot(lhs, rhs, preferred_element_type=F32)
+    n = place[k]
+    gate = acc[:, :LANES] * gs_ref[pl.ds(n, 1), :]
+    up_part = acc[:, LANES:] * us_ref[pl.ds(n, 1), :]
+    out[here, k * LANES : (k + 1) * LANES] = (gate / (1.0 + jnp.exp(-gate)) * up_part).astype(BF)
 
 
 def hidden_units(config, place, normed, w_up, gs_ref, us_ref, out):
@@ -182,104 +201,103 @@
         here = pl.ds(pl.multiple_of(i * chunk, chunk), chunk)
         lhs = normed[here, :]
         for k in range(tiles):
-            rhs = flat(w_up, slice(2 * k * LANES, (2 * k + 2) * LANES))
-            acc = jnp.dot(lhs, rhs, preferred_element_type=F32)
-            n = place[k]
-            gate = acc[:, :LANES] * gs_ref[pl.ds(n, 1), :]
-            up_part = acc[:, LANES:] * us_ref[pl.ds(n, 1), :]
-            out[here, k * LANES : (k + 1) * LANES] = (gate / (1.0 + jnp.exp(-gate)) * up_part).astype(BF)
-
-
-def feed_forward(config, ids, state, gain, stages, pieces, scales, last):
+            hidden_tile(k, place, lhs, w_up, gs_ref, us_ref, out, here)
+
+
+def down_block(left, weight, l):
+    acc = jnp.dot(left, weight[l, SPARE:, :], preferred_element_type=F32)
+    terms = weight[l, :SPARE, :].astype(F32)
+    return (acc * (terms[0:1] + terms[1:2] + terms[2:3])).astype(BF)
+
+
+def second_pass(config, ids, state, gain, stages, pieces, scales):
     blocks, tiles, chunk, place_of = config["blocks"], config["tiles"], config["chunk"], config["place"]
     count, width = state[0].shape
-    columns = width // blocks
-    units = tiles * LANES
-    n_state = len(state)
+    columns, units, half = width // blocks, tiles * LANES, width // 2
     n_copies = sum(len(stage.runs()) for stage in stages)
+    chunks, step = count // chunk, 16
 
     def body(*refs):
         at, place, refs = refs[0], refs[1], refs[2:]
-        sources, refs = refs[:n_state], refs[n_state:]
-        gain_ref, gs_ref, us_ref, refs = refs[0], refs[1], refs[2], refs[3:]
+        sources, gain_ref, gs_ref, us_ref, refs = refs[:3], refs[3], refs[4], refs[5], refs[6:]
         parts = [refs[N_PIECES * i : N_PIECES * (i + 1)] for i in range(len(stages))]
         refs = refs[N_PIECES * len(stages) :]
-        n_out = 3 if last else len(state[:2])
-        outs, refs = refs[:n_out], refs[n_out:]
-        w_up, w_down, normed, hidden, sems, refs = refs[0], refs[1], refs[2], refs[3], refs[4], refs[5:]
-        st, refs = refs[:n_state], refs[n_state:]
-        loads = [pltpu.make_async_copy(a, b, sems.at[n_copies + k]) for k, (a, b) in enumerate(zip(sources, st))]
-        up = fetches(stages[0], parts[0], w_up, sems, 0)
-        up += fetches(stages[1], parts[1], w_up, sems, len(up))
-        down = fetches(stages[2], parts[2], w_down, sems, len(up))
-        for copy in loads + up + down:
-            copy.start()
+        outs, refs = refs[:3], refs[3:]
+        w_up, w_down, normed, hidden, new_ref, halves, rests, sems, load_sems, save_sems = refs[:10]
+        st = refs[10:]
+        rows = [pl.ds(i * chunk, chunk) for i in range(chunks)]
+        loads = [
+            [pltpu.make_async_copy(a.at[r, :], b.at[r, :], load_sems.at[3 * i + k]) for k, (a, b) in enumerate(zip(sources, st))]
+            for i, r in enumerate(rows)
+        ]
+        copies, at_sem = [], 0
+        for stage, part, scratch in zip(stages, parts, (w_up, w_up, w_down)):
+            copies.append(fetches(stage, part, scratch, sems, at_sem))
+            at_sem += len(copies[-1])
+        for group in [loads[0], copies[0], copies[1]] + loads[1:] + [copies[2]]:
+            for copy in group:
+                copy.start()
         gains = local_gain(gain_ref, at, blocks)
-        for copy in loads:
+        for copy in loads[0]:
             copy.wait()
-        residual_and_norm(st[0], 0.5 if not last else 1.0, st[1:], gains, st[0], normed, 16)
+        residual_and_norm(st[0], 1.0, st[1:], gains, new_ref, normed, step, 0, chunk)
         saves = []
-        if n_state > 1 and not last:
-            saves.append(pltpu.make_async_copy(st[0], outs[1], sems.at[n_copies + 3]))
-            saves[0].start()
-        for copy in up:
-            copy.wait()
-
-        hidden_units(config, place, normed, w_up, gs_ref, us_ref, hidden)
-
-        for copy in down:
-            copy.wait()
-        halves, rests = refs if last else (refs[0], None)
-
-        @pl.loop(0, count // chunk)
-        def _(i):
-            here = pl.ds(pl.multiple_of(i * chunk, chunk), chunk)
+        for i in range(chunks):
+            here = slice(i * chunk, (i + 1) * chunk)
+            pending = []
+            if i + 1 < chunks:
+                pending = list(range((i + 1) * chunk, (i + 2) * chunk, step))
+                for copy in loads[i + 1]:
+                    copy.wait()
+            done = 0
+            for s in range(2):
+                if i == 0:
+                    for copy in copies[s]:
+                        copy.wait()
+                for k in stages[s].tiles:
+                    hidden_tile(k, place, normed[here, :], w_up, gs_ref, us_ref, hidden, here)
+                    done += 1
+                    share = -(-len(pending) // (tiles - done + 1))
+                    for row in pending[:share]:
+                        norm_block(st[0], 1.0, st[1:], gains, new_ref, normed, row, step)
+                    pending = pending[share:]
+            if i == 0:
+                for copy in copies[2]:
+                    copy.wait()
             left = hidden[here, :]
             for l in range(blocks):
-                acc = jnp.dot(left, w_down[l, SPARE:, :], preferred_element_type=F32)
-                terms = w_down[l, :SPARE, :].astype(F32)
-                value = (acc * (terms[0:1] + terms[1:2] + terms[2:3])).astype(BF)
-                block = slice(l * columns, (l + 1) * columns)
-                if not last:
-                    halves[here, block] = value
-                else:
-                    j = at[l]
-                    side = jnp.where(lax.div(j, blocks // 2) == at[blocks], 0, 1)
-                    there = pl.ds(pl.multiple_of(lax.rem(j, blocks // 2) * columns, columns), columns)
-                    halves[side, here, there] = value
-                    rests[side, here, there] = st[0][here, block]
-
-        if last:
+                value = down_block(left, w_down, l)
+                j = at[l]
+                side = jnp.where(lax.div(j, blocks // 2) == at[blocks], 0, 1)
+                there = pl.ds(pl.multiple_of(lax.rem(j, blocks // 2) * columns, columns), columns)
+                halves[side, here, there] = value
+                rests[side, here, there] = new_ref[here, l * columns : (l + 1) * columns]
             results = ((halves.at[1], outs[1]), (halves.at[0], outs[0]), (rests.at[0], outs[2]))
-        else:
-            results = ((halves, outs[0]),)
-        results = [pltpu.make_async_copy(a, b, sems.at[n_copies + 4 + k]) for k, (a, b) in enumerate(results)]
-        for copy in results:
-            copy.start()
-        for copy in results + saves:
+            for k, (a, b) in enumerate(results):
+                saves.append(pltpu.make_async_copy(a.at[rows[i], :], b.at[rows[i], :], save_sems.at[3 * i + k]))
+                saves[-1].start()
+        for copy in saves:
             copy.wait()
 
-    if last:
-        shapes = [jax.ShapeDtypeStruct((count, width // 2), BF)] * 3
-        extra = [pltpu.VMEM((2, count, width // 2), BF)] * 2
-    else:
-        shapes = [jax.ShapeDtypeStruct((count, width), BF)] * len(state[:2])
-        extra = [pltpu.VMEM((count, width), BF)]
     return pl.pallas_call(
         body,
-        out_shape=shapes,
-        in_specs=[SMEM, SMEM] + [HBM] * n_state + [VMEM] * 3 + [HBM] * (N_PIECES * len(stages)),
-        out_specs=[HBM] * len(shapes),
+        out_shape=[jax.ShapeDtypeStruct((count, half), BF)] * 3,
+        in_specs=[SMEM, SMEM] + [ANY] * 3 + [VMEM] * 3 + [HBM] * (N_PIECES * len(stages)),
+        out_specs=[ANY] * 3,
         scratch_shapes=[
             pltpu.VMEM((blocks, columns, 2 * units), BF),
             pltpu.VMEM((blocks, SPARE + units, columns), BF),
             pltpu.VMEM((count, width), BF),
             pltpu.VMEM((count, units), BF),
-            pltpu.SemaphoreType.DMA((n_copies + 8,)),
+            pltpu.VMEM((count, width), BF),
+            pltpu.VMEM((2, count, half), BF),
+            pltpu.VMEM((2, count, half), BF),
+            pltpu.SemaphoreType.DMA((n_copies,)),
+            pltpu.SemaphoreType.DMA((3 * chunks,)),
+            pltpu.SemaphoreType.DMA((3 * chunks,)),
         ]
-        + [pltpu.VMEM((count, width), BF)] * n_state
-        + extra,
-        compiler_params=params(),
+        + [pltpu.VMEM((count, width), BF)] * 3,
+        compiler_params=params(55),
         cost_estimate=cost(6 * count * width * units, 2 * 3 * width * units),
     )(
         ids,
@@ -325,7 +343,7 @@
             pltpu.SemaphoreType.DMA((n_copies + 1,)),
             pltpu.VMEM((count, width), BF),
         ],
-        compiler_params=params(),
+        compiler_params=params(24),
         cost_estimate=cost(4 * count * width * units, 2 * 2 * width * units),
     )(
         ids,
@@ -357,9 +375,7 @@
             here = pl.ds(pl.multiple_of(i * chunk, chunk), chunk)
             left = left_ref[here, :]
             for l in range(blocks):
-                acc = jnp.dot(left, w_down[l, SPARE:, :], preferred_element_type=F32)
-                terms = w_down[l, :SPARE, :].astype(F32)
-                out[here, l * columns : (l + 1) * columns] = (acc * (terms[0:1] + terms[1:2] + terms[2:3])).astype(BF)
+                out[here, l * columns : (l + 1) * columns] = down_block(left, w_down, l)
 
     return pl.pallas_call(
         body,
@@ -367,7 +383,7 @@
         in_specs=[VMEM] + [HBM] * N_PIECES,
         out_specs=VMEM,
         scratch_shapes=[pltpu.VMEM((blocks, SPARE + units, columns), BF), pltpu.SemaphoreType.DMA((n_copies,))],
-        compiler_params=params(),
+        compiler_params=params(16),
         cost_estimate=cost(2 * count * width * units, 2 * width * units),
     )(hidden, *pieces)
 
@@ -381,28 +397,35 @@
     count, width = state[0].shape
     columns = width // blocks
     n_copies = len(stage.runs())
+    chunks, step = count // chunk, 16
 
     def body(*refs):
         at, place, refs = refs[0], refs[1], refs[2:]
         sources, gain_ref, us_ref, vs_ref = refs[:3], refs[3], refs[4], refs[5]
         parts, refs = refs[6 : 6 + N_PIECES], refs[6 + N_PIECES :]
-        new_out, u_out, v_out, sum_out, w, normed, sems, *st = refs
-        loads = [pltpu.make_async_copy(a, b, sems.at[n_copies + k]) for k, (a, b) in enumerate(zip(sources, st))]
+        new_out, u_out, v_out, sum_out, w, normed, sems, load_sems, *st = refs
+        rows = [pl.ds(i * chunk, chunk) for i in range(chunks)]
+        loads = [
+            [pltpu.make_async_copy(a.at[r, :], b.at[r, :], load_sems.at[3 * i + k]) for k, (a, b) in enumerate(zip(sources, st))]
+            for i, r in enumerate(rows)
+        ]
         copies = fetches(stage, parts, w, sems, 0)
-        for copy in loads + copies:
-            copy.start()
+        for group in [loads[0], copies] + loads[1:]:
+            for copy in group:
+                copy.start()
         gains = local_gain(gain_ref, at, blocks)
-        for copy in loads:
+        for copy in loads[0]:
             copy.wait()
-        residual_and_norm(st[0], 0.5, st[1:], gains, st[0], normed, 16)
-        save = pltpu.make_async_copy(st[0], new_out, sems.at[n_copies + 3])
-        save.start()
+        residual_and_norm(st[0], 0.5, st[1:], gains, new_out, normed, step, 0, chunk)
         for copy in copies:
             copy.wait()
-
-        @pl.loop(0, count // chunk)
-        def _(i):
-            here = pl.ds(pl.multiple_of(i * chunk, chunk), chunk)
+        for i in range(chunks):
+            here = slice(i * chunk, (i + 1) * chunk)
+            pending = []
+            if i + 1 < chunks:
+                pending = list(range((i + 1) * chunk, (i + 2) * chunk, step))
+                for copy in loads[i + 1]:
+                    copy.wait()
             lhs = normed[here, :]
             plain = jnp.zeros((chunk, LANES), F32)
             square = jnp.zeros((chunk, LANES), F32)
@@ -416,12 +439,14 @@
                 v_out[here, block] = v_act
                 plain += v_act
                 square += v_act * v_act
+                share = -(-len(pending) // (tiles - k))
+                for row in pending[:share]:
+                    norm_block(st[0], 0.5, st[1:], gains, new_out, normed, row, step)
+                pending = pending[share:]
             index = lax.broadcasted_iota(jnp.int32, (chunk, LANES), 1)
             sum_out[here, :] = jnp.where(
                 index == 0, jnp.sum(plain, axis=1, keepdims=True), jnp.sum(square, axis=1, keepdims=True)
             )
-
-        save.wait()
 
     return pl.pallas_call(
         body,
@@ -431,15 +456,16 @@
             jax.ShapeDtypeStruct((count, tiles * LANES), F32),
             jax.ShapeDtypeStruct((count, LANES), F32),
         ],
-        in_specs=[SMEM, SMEM] + [HBM] * 3 + [VMEM] * 3 + [HBM] * N_PIECES,
-        out_specs=[HBM] + [VMEM] * 3,
+        in_specs=[SMEM, SMEM] + [ANY] * 3 + [VMEM] * 3 + [HBM] * N_PIECES,
+        out_specs=[VMEM] * 4,
         scratch_shapes=[
             pltpu.VMEM((blocks, columns, 2 * tiles * LANES), BF),
             pltpu.VMEM((count, width), BF),
-            pltpu.SemaphoreType.DMA((n_copies + 4,)),
+            pltpu.SemaphoreType.DMA((n_copies,)),
+            pltpu.SemaphoreType.DMA((3 * chunks,)),
         ]
         + [pltpu.VMEM((count, width), BF)] * 3,
-        compiler_params=params(),
+        compiler_params=params(48),
         cost_estimate=cost(4 * count * width * tiles * LANES, 4 * width * tiles * LANES),
     )(
         ids,
@@ -492,9 +518,7 @@
             here = pl.ds(pl.multiple_of(i * chunk, chunk), chunk)
             left = mixed[here, :]
             for l in range(blocks):
-                acc = jnp.dot(left, w_out[l, SPARE:, :], preferred_element_type=F32)
-                terms = w_out[l, :SPARE, :].astype(F32)
-                out[here, l * columns : (l + 1) * columns] = (acc * (terms[0:1] + terms[1:2] + terms[2:3])).astype(BF)
+                out[here, l * columns : (l + 1) * columns] = down_block(left, w_out, l)
 
     return pl.pallas_call(
         body,
@@ -506,7 +530,7 @@
             pltpu.VMEM((count, channels), BF),
             pltpu.SemaphoreType.DMA((n_copies,)),
         ],
-        compiler_params=params(),
+        compiler_params=params(50),
         cost_estimate=cost(2 * count * width * channels, 2 * width * channels),
     )(
         config["place"],
@@ -532,7 +556,7 @@
         out_shape=[jax.ShapeDtypeStruct(shape, BF) for shape in shapes],
         in_specs=[SMEM] + [VMEM] * len(values),
         out_specs=[VMEM] * len(shapes),
-        compiler_params=params(),
+        compiler_params=params(12),
         cost_estimate=cost(1000000, 4 * sum(v.size for v in values)),
     )(flag, *values)
 
@@ -643,8 +667,8 @@
     sums_in = lax.ppermute(sums, "tp", SWAP)
     mixed = mixer_out(mix, u_act, v_act, sums, sums_in, (ln_gain, ln_bias), spatial_weight, spatial_bias, ou, pieces["ou"])
     mixed_in = lax.ppermute(mixed, "tp", SWAP)
-    own_last, send, rest = feed_forward(
-        ff, ids, (middle, mixed, mixed_in), norm_second, ff_stages, ff_pieces, (gate_scale, up_scale), True)
+    own_last, send, rest = second_pass(
+        ff, ids, (middle, mixed, mixed_in), norm_second, ff_stages, ff_pieces, (gate_scale, up_scale))
     got = lax.ppermute(send, "tp", SWAP)
     return (rest.astype(F32) + 0.5 * (own_last.astype(F32) + got.astype(F32))).astype(BF)
 

time: 433 us -> 418 us (0.965)
  Pallas kernels: 126 us -> 79.2 us
  waiting for transfers between devices: 187 us -> 223 us
  local copies, waits for them, and re-layouts: 22.5 us -> 17.2 us
    pallas_call x20, Pallas kernels: 48.6 us -> 14.3 us  [join(): pl.pallas_call(body, out_shape=[jax.ShapeDtypeStruct(shape, BF) for shape...]
    ppermute x5, waiting for transfers between devices: 19 us -> 36.5 us  [gather(): y = lax.ppermute(y, 'fs', across)]
    ppermute x5, waiting for transfers between devices: 18 us -> 27.1 us  [gather(): p = lax.ppermute(p, 'rep', SWAP)]
    ppermute x5, waiting for transfers between devices: 32.2 us -> 39.7 us  [gather(): r = lax.ppermute(r, 'fs', across)]
    unnamed x63 -> x145, local copies, waits for them, and re-layouts: 17.8 us -> 15.7 us
  transfers between devices with their start and end apart: 40 -> 40, of which waited for: 20 -> 22; matrix products, arithmetic and copies ran while one was open for 3% -> 1% of each run, Pallas kernels for 21% -> 11%
where the time goes in v1:
time: 418 us; the launch traced here: 417 us
  waiting for transfers between devices  223 us (53%)
  starting transfers between devices  89.1 us (21%)
  Pallas kernels  79.2 us (19%)
  local copies, waits for them, and re-layouts  17.2 us (4%)
  other arithmetic  7.19 us (2%)
    ppermute x5, waiting for transfers between devices, gather(): e = lax.ppermute(near, 'fs', pairs([(0, 1), (1, 0), (2, 3), (3, 2)]))  73.8 us
    ppermute x5, starting transfers between devices, gather(): e = lax.ppermute(near, 'fs', pairs([(0, 1), (1, 0), (2, 3), (3, 2)]))  55.3 us
    ppermute x5, waiting for transfers between devices, gather(): r = lax.ppermute(r, 'fs', across)  39.7 us
    ppermute x5, waiting for transfers between devices, gather(): y = lax.ppermute(y, 'fs', across)  36.5 us
    ppermute x5, waiting for transfers between devices, gather(): p = lax.ppermute(p, 'rep', SWAP)  27.1 us
    pallas_call x1, Pallas kernels, second_pass(): pl.pallas_call(body, out_shape=[jax.ShapeDtypeStruct((count, half), BF)]...  25.3 us
    ppermute x5, waiting for transfers between devices, gather(): g = lax.ppermute(m, 'fs', pairs([(1, 0), (2, 3)]))  22.3 us
    unnamed x145, local copies, waits for them, and re-layouts  15.7 us
  transfers between devices with their start and end apart: 40, of which 22 were waited for; matrix products, arithmetic and copies ran while one was open for 1% of the time, Pallas kernels for 11%

profile of v1, /device:TPU:0, one launch (start us, length us, event | category | flops | bytes accessed | tf_op | source)
XLA Modules:
  0.0 416.8 jit_solution(18292600581710846696)
XLA Ops:
  7.4 14.7 %collective-permute-done.8.e_ref.refs_9_.refs_17_ = bf16[1,256,1280]{2,1,0:T(8,128)(2,1)S(1)} collective-permute-done((bf16[1,256,1280]{2,1,0:T(8,128)(2,1)S(1)}, bf16[1,256,1280]{2,1,0:T(8,128)(2,1)S(1)}, u32[]{:S(2)}, u32[]{:S(2)}) %collective-permute-start.8) | collective-permute-done | bytes 655392 | tf_op jit(solution)/shard_map/ppermute | solution.py:608
  24.7 4.5 %collective-permute-start.15 = (bf16[1,1168,256]{2,1,0:T(8,128)(2,1)S(1)}, bf16[1,1168,256]{2,1,0:T(8,128)(2,1)S(1)}, u32[]{:S(2)}, u32[]{:S(2)}) collective-permute-start(bf16[1,1168,256]{2,1,0:T(8,128)(2,1)S(1)} %get-tuple-element.54.near_ref.refs_0_.refs_24_), channel_id=1, source_target_pairs={{0,4},{2,6},{4,0},{6,2},{8,12},{10,14},{12,8},{14,10},{1,5},{3,7},... | collective-permute-start | bytes 1794056 | tf_op jit(solution)/shard_map/ppermute | solution.py:608
  29.4 14.2 %collective-permute-done.15.e_ref.refs_1_.refs_25_ = bf16[1,1168,256]{2,1,0:T(8,128)(2,1)S(1)} collective-permute-done((bf16[1,1168,256]{2,1,0:T(8,128)(2,1)S(1)}, bf16[1,1168,256]{2,1,0:T(8,128)(2,1)S(1)}, u32[]{:S(2)}, u32[]{:S(2)}) %collective-permute-start.15) | collective-permute-done | bytes 598048 | tf_op jit(solution)/shard_map/ppermute | solution.py:608
  45.3 7.5 %collective-permute-done.1.e_ref.refs_1_.refs_9_ = bf16[1,256,1024]{2,1,0:T(8,128)(2,1)S(1)} collective-permute-done((bf16[1,256,1024]{2,1,0:T(8,128)(2,1)S(1)}, bf16[1,256,1024]{2,1,0:T(8,128)(2,1)S(1)}, u32[]{:S(2)}, u32[]{:S(2)}) %collective-permute-start.1) | collective-permute-done | bytes 524320 | tf_op jit(solution)/shard_map/ppermute | solution.py:608
  61.5 47.5 %collective-permute-start.23 = (bf16[1,256,768]{2,1,0:T(8,128)(2,1)S(1)}, bf16[1,256,768]{2,1,0:T(8,128)(2,1)S(1)}, u32[]{:S(2)}, u32[]{:S(2)}) collective-permute-start(bf16[1,256,768]{2,1,0:T(8,128)(2,1)S(1)} %get-tuple-element.60.near_ref.refs_8_), channel_id=1, source_target_pairs={{0,4},{2,6},{4,0},{6,2},{8,12},{10,14},{12,8},{14,10},{1,5},{3,7},... | collective-permute-start | bytes 1179656 | tf_op jit(solution)/shard_map/ppermute | solution.py:608
  110.8 31.6 %collective-permute-done.23.e_ref.refs_9_ = bf16[1,256,768]{2,1,0:T(8,128)(2,1)S(1)} collective-permute-done((bf16[1,256,768]{2,1,0:T(8,128)(2,1)S(1)}, bf16[1,256,768]{2,1,0:T(8,128)(2,1)S(1)}, u32[]{:S(2)}, u32[]{:S(2)}) %collective-permute-start.23) | collective-permute-done | bytes 393248 | tf_op jit(solution)/shard_map/ppermute | solution.py:608
  156.0 7.1 %collective-permute-done.4.y_ref.refs_4_.refs_12_ = bf16[2,256,768]{2,1,0:T(8,128)(2,1)} collective-permute-done((bf16[2,256,768]{2,1,0:T(8,128)(2,1)}, bf16[2,256,768]{2,1,0:T(8,128)(2,1)}, u32[]{:S(2)}, u32[]{:S(2)}) %collective-permute-start.4) | collective-permute-done | bytes 786464 | tf_op jit(solution)/shard_map/ppermute | solution.py:611
  169.4 10.5 %collective-permute-done.11.y_ref.refs_12_.refs_20_ = bf16[2,256,768]{2,1,0:T(8,128)(2,1)} collective-permute-done((bf16[2,256,768]{2,1,0:T(8,128)(2,1)}, bf16[2,256,768]{2,1,0:T(8,128)(2,1)}, u32[]{:S(2)}, u32[]{:S(2)}) %collective-permute-start.11) | collective-permute-done | bytes 786464 | tf_op jit(solution)/shard_map/ppermute | solution.py:611
  182.7 31.2 %collective-permute-done.5.r_ref.refs_5_.refs_13_ = bf16[2,256,768]{2,1,0:T(8,128)(2,1)} collective-permute-done((bf16[2,256,768]{2,1,0:T(8,128)(2,1)}, bf16[2,256,768]{2,1,0:T(8,128)(2,1)}, u32[]{:S(2)}, u32[]{:S(2)}) %collective-permute-start.5) | collective-permute-done | bytes 786464 | tf_op jit(solution)/shard_map/ppermute | solution.py:616
  219.1 7.7 %collective-permute-done.18.y_ref.refs_4_.refs_28_ = bf16[2,784,256]{2,1,0:T(8,128)(2,1)S(1)} collective-permute-done((bf16[2,784,256]{2,1,0:T(8,128)(2,1)S(1)}, bf16[2,784,256]{2,1,0:T(8,128)(2,1)S(1)}, u32[]{:S(2)}, u32[]{:S(2)}) %collective-permute-start.18) | collective-permute-done | bytes 802848 | tf_op jit(solution)/shard_map/ppermute | solution.py:611
  233.9 14.5 %collective-permute-done.7.refs_7_.refs_15_ = bf16[2,256,768]{2,1,0:T(8,128)(2,1)S(1)} collective-permute-done((bf16[2,256,768]{2,1,0:T(8,128)(2,1)S(1)}, bf16[2,256,768]{2,1,0:T(8,128)(2,1)S(1)}, u32[]{:S(2)}, u32[]{:S(2)}) %collective-permute-start.7) | collective-permute-done | bytes 786464 | tf_op jit(solution)/shard_map/ppermute | solution.py:618
  248.6 11.5 %shard_map.199.left_ref = bf16[640,1408]{1,0:T(8,128)(2,1)S(1)} custom-call(s32[9]{0:T(128)S(1)} %copy-done.42, s32[11]{0:T(128)S(1)} %broadcast_select_fusion.1.at.place.refs_1_, bf16[640,2048]{1,0:T(8,128)(2,1)S(1)} %dynamic-slice_dynamic-update-slice_fusion.source.refs_2_, f32[8,256]{1,0:T(8,128)S(1)} %reshape.41.gain_ref, f32[11,128]{1,0:T(8,128)S(1)} %bitcast.25, ...), custom_call_target="tpu_custom_call" | custom-call | flops 7381975040 | bytes 11534336 | tf_op jit(solution)/shard_map/pallas_call | solution.py:335
  260.2 15.5 %collective-permute-done.20.refs_6_.refs_30_ = bf16[1,1536,256]{2,1,0:T(8,128)(2,1)S(1)} collective-permute-done((bf16[1,1536,256]{2,1,0:T(8,128)(2,1)S(1)}, bf16[1,1536,256]{2,1,0:T(8,128)(2,1)S(1)}, u32[]{:S(2)}, u32[]{:S(2)}) %collective-permute-start.20) | collective-permute-done | bytes 786464 | tf_op jit(solution)/shard_map/ppermute | solution.py:614
  275.7 8.5 %shard_map.205.refs_3_ = bf16[640,2048]{1,0:T(8,128)(2,1)} custom-call(bf16[640,1408]{1,0:T(8,128)(2,1)S(1)} %shard_map.199.left_ref, bf16[1,1168,256]{2,1,0:T(8,128)(2,1)S(1)} %copy-done.27, bf16[1,1168,256]{2,1,0:T(8,128)(2,1)S(1)} %copy-done.4, bf16[2,1168,256]{2,1,0:T(8,128)(2,1)S(1)} %copy-done.15, bf16[1,256,256]{2,1,0:T(8,128)(2,1)S(1)} %copy-done.61, ...), custom_call_target="tpu_custom_call" | custom-call | flops 3690987520 | bytes 5767168 | tf_op jit(solution)/shard_map/pallas_call | solution.py:380
  285.8 20.3 %collective-permute-done.25.g_ref = bf16[2,256,768]{2,1,0:T(8,128)(2,1)S(1)} collective-permute-done((bf16[2,256,768]{2,1,0:T(8,128)(2,1)S(1)}, bf16[2,256,768]{2,1,0:T(8,128)(2,1)S(1)}, u32[]{:S(2)}, u32[]{:S(2)}) %collective-permute-start.25) | collective-permute-done | bytes 786464 | tf_op jit(solution)/shard_map/ppermute | solution.py:612
  309.1 5.7 %collective-permute-done.31.e_ref.refs_10_ = bf16[1,400,256]{2,1,0:T(8,128)(2,1)S(1)} collective-permute-done((bf16[1,400,256]{2,1,0:T(8,128)(2,1)S(1)}, bf16[1,400,256]{2,1,0:T(8,128)(2,1)S(1)}, u32[]{:S(2)}, u32[]{:S(2)}) %collective-permute-start.31) | collective-permute-done | bytes 204832 | tf_op jit(solution)/shard_map/ppermute | solution.py:608
  316.3 4.8 %collective-permute-done.27.r_ref.refs_13_ = bf16[2,256,512]{2,1,0:T(8,128)(2,1)S(1)} collective-permute-done((bf16[2,256,512]{2,1,0:T(8,128)(2,1)S(1)}, bf16[2,256,512]{2,1,0:T(8,128)(2,1)S(1)}, u32[]{:S(2)}, u32[]{:S(2)}) %collective-permute-start.27) | collective-permute-done | bytes 524320 | tf_op jit(solution)/shard_map/ppermute | solution.py:616
  324.9 6.1 %collective-permute-done.26.y_ref.refs_12_ = bf16[2,256,512]{2,1,0:T(8,128)(2,1)S(1)} collective-permute-done((bf16[2,256,512]{2,1,0:T(8,128)(2,1)S(1)}, bf16[2,256,512]{2,1,0:T(8,128)(2,1)S(1)}, u32[]{:S(2)}, u32[]{:S(2)}) %collective-permute-start.26) | collective-permute-done | bytes 524320 | tf_op jit(solution)/shard_map/ppermute | solution.py:611
  338.0 5.1 %collective-permute-done.34.y_ref.refs_13_ = bf16[2,272,256]{2,1,0:T(8,128)(2,1)S(1)} collective-permute-done((bf16[2,272,256]{2,1,0:T(8,128)(2,1)}, bf16[2,272,256]{2,1,0:T(8,128)(2,1)S(1)}, u32[]{:S(2)}, u32[]{:S(2)}) %collective-permute-start.34) | collective-permute-done | bytes 278560 | tf_op jit(solution)/shard_map/ppermute | solution.py:611
  348.4 8.5 %collective-permute-done.28.refs_14_ = bf16[1,256,1280]{2,1,0:T(8,128)(2,1)} collective-permute-done((bf16[1,256,1280]{2,1,0:T(8,128)(2,1)}, bf16[1,256,1280]{2,1,0:T(8,128)(2,1)}, u32[]{:S(2)}, u32[]{:S(2)}) %collective-permute-start.28) | collective-permute-done | bytes 655392 | tf_op jit(solution)/shard_map/ppermute | solution.py:614
  357.9 9.7 %shard_map.211 = (bf16[640,2048]{1,0:T(8,128)(2,1)}, f32[640,512]{1,0:T(8,128)S(1)}, f32[640,512]{1,0:T(8,128)}, f32[640,128]{1,0:T(8,128)S(1)}) custom-call(s32[9]{0:T(128)S(1)} %copy-done.43, s32[4]{0:T(128)S(1)} %broadcast_select_fusion.at.refs_1_.refs_0_, bf16[640,2048]{1,0:T(8,128)(2,1)} %copy-done, bf16[640,2048]{1,0:T(8,128)(2,1)} %shard_map.205.refs_3_, ...), custom_call_target="tpu_custom_call" | custom-call | flops 2684354560 | bytes 4194304 | tf_op jit(solution)/shard_map/pallas_call | solution.py:451
  370.6 7.2 %shard_map.217.refs_3_ = bf16[640,2048]{1,0:T(8,128)(2,1)} custom-call(s32[4]{0:T(128)S(1)} %broadcast_select_fusion.at.refs_1_.refs_0_, f32[640,512]{1,0:T(8,128)} %copy-done.13, f32[640,512]{1,0:T(8,128)} %get-tuple-element.68.refs_2_, f32[640,128]{1,0:T(8,128)S(1)} %get-tuple-element.69.refs_3_, f32[640,128]{1,0:T(8,128)S(1)} %collective-permute-done.30.refs_4_, ...), custom_call_target="tpu_custom_call" | custom-call | flops 1342177280 | bytes 2097152 | tf_op jit(solution)/shard_map/pallas_call | solution.py:523
  378.6 4.4 %collective-permute-done.38.refs_4_ = bf16[640,2048]{1,0:T(8,128)(2,1)S(1)} collective-permute-done((bf16[640,2048]{1,0:T(8,128)(2,1)}, bf16[640,2048]{1,0:T(8,128)(2,1)S(1)}, u32[]{:S(2)}, u32[]{:S(2)}) %collective-permute-start.38) | collective-permute-done | bytes 2621472 | tf_op jit(solution)/shard_map/ppermute | solution.py:669
  384.6 25.3 %shard_map.218 = (bf16[640,1024]{1,0:T(8,128)(2,1)}, bf16[640,1024]{1,0:T(8,128)(2,1)}, bf16[640,1024]{1,0:T(8,128)(2,1)}) custom-call(s32[9]{0:T(128)} %stack.39.at.refs_0_, s32[11]{0:T(128)} %copy-done.41, bf16[640,2048]{1,0:T(8,128)(2,1)} %get-tuple-element.66.refs_2_, bf16[640,2048]{1,0:T(8,128)(2,1)} %shard_map.217.refs_3_, ...), custom_call_target="tpu_custom_call" | custom-call | flops 11072962560 | bytes 17301504 | tf_op jit(solution)/shard_map/pallas_call | solution.py:282
  (240 shorter events, 91.8 us)
Async XLA Ops:
  23.3 31.4 %collective-permute-start.9 = (bf16[2,256,1280]{2,1,0:T(8,128)(2,1)S(1)}, bf16[2,256,1280]{2,1,0:T(8,128)(2,1)S(1)}, u32[]{:S(2)}, u32[]{:S(2)}) collective-permute-start(bf16[2,256,1280]{2,1,0:T(8,128)(2,1)S(1)} %get-tuple-element.49), channel_id=1, source_target_pairs={{4,8},{6,10},{8,4},{10,6},{5,9},{7,11},{9,5},{11,7},{20,24},{22,26... | collective-permute-start | bytes 3932168 | tf_op jit(solution)/shard_map/ppermute | solution.py:610
  29.3 23.6 %collective-permute-start.1 = (bf16[1,256,1024]{2,1,0:T(8,128)(2,1)S(1)}, bf16[1,256,1024]{2,1,0:T(8,128)(2,1)S(1)}, u32[]{:S(2)}, u32[]{:S(2)}) collective-permute-start(bf16[1,256,1024]{2,1,0:T(8,128)(2,1)S(1)} %copy-done.32), channel_id=1, source_target_pairs={{0,4},{2,6},{4,0},{6,2},{8,12},{10,14},{12,8},{14,10},{1,5},{3,7},... | collective-permute-start | bytes 1572872 | tf_op jit(solution)/shard_map/ppermute | solution.py:608
  54.6 54.4 %collective-permute-start.10 = (bf16[2,256,1280]{2,1,0:T(8,128)(2,1)S(1)}, bf16[2,256,1280]{2,1,0:T(8,128)(2,1)S(1)}, u32[]{:S(2)}, u32[]{:S(2)}) collective-permute-start(bf16[2,256,1280]{2,1,0:T(8,128)(2,1)S(1)} %collective-permute-done.9.m_ref), channel_id=1, source_target_pairs={{4,0},{6,2},{8,12},{10,14},{5,1},{7,3},{9,13},{11,15},{20,16},{22,... | collective-permute-start | bytes 3932168 | tf_op jit(solution)/shard_map/ppermute | solution.py:612
  56.0 87.9 %collective-permute-start.17 = (bf16[2,1168,256]{2,1,0:T(8,128)(2,1)S(1)}, bf16[2,1168,256]{2,1,0:T(8,128)(2,1)S(1)}, u32[]{:S(2)}, u32[]{:S(2)}) collective-permute-start(bf16[2,1168,256]{2,1,0:T(8,128)(2,1)S(1)} %collective-permute-done.16.m_ref), channel_id=1, source_target_pairs={{4,0},{6,2},{8,12},{10,14},{5,1},{7,3},{9,13},{11,15},{20,16},{22,... | collective-permute-start | bytes 3588104 | tf_op jit(solution)/shard_map/ppermute | solution.py:612
  57.3 89.2 %collective-permute-start.3 = (bf16[2,256,1024]{2,1,0:T(8,128)(2,1)S(1)}, bf16[2,256,1024]{2,1,0:T(8,128)(2,1)S(1)}, u32[]{:S(2)}, u32[]{:S(2)}) collective-permute-start(bf16[2,256,1024]{2,1,0:T(8,128)(2,1)S(1)} %collective-permute-done.2.m_ref), channel_id=1, source_target_pairs={{4,0},{6,2},{8,12},{10,14},{5,1},{7,3},{9,13},{11,15},{20,16},{22,... | collective-permute-start | bytes 3145736 | tf_op jit(solution)/shard_map/ppermute | solution.py:612
  58.6 94.8 %collective-permute-start = (bf16[640,1024]{1,0:T(8,128)(2,1)}, bf16[640,1024]{1,0:T(8,128)(2,1)}, u32[]{:S(2)}, u32[]{:S(2)}) collective-permute-start(bf16[640,1024]{1,0:T(8,128)(2,1)} %param.20), channel_id=1, source_target_pairs={{0,1},{1,0},{2,3},{3,2},{4,5},{5,4},{6,7},{7,6},{8,9},{9,8},{10,11... | collective-permute-start | bytes 3932168 | tf_op jit(solution)/shard_map/ppermute | solution.py:655
  61.5 80.8 %collective-permute-start.23 = (bf16[1,256,768]{2,1,0:T(8,128)(2,1)S(1)}, bf16[1,256,768]{2,1,0:T(8,128)(2,1)S(1)}, u32[]{:S(2)}, u32[]{:S(2)}) collective-permute-start(bf16[1,256,768]{2,1,0:T(8,128)(2,1)S(1)} %get-tuple-element.60.near_ref.refs_8_), channel_id=1, source_target_pairs={{0,4},{2,6},{4,0},{6,2},{8,12},{10,14},{12,8},{14,10},{1,5},{3,7},... | collective-permute-start | bytes 1179656 | tf_op jit(solution)/shard_map/ppermute | solution.py:608
  109.2 40.8 %collective-permute-start.12 = (bf16[2,256,768]{2,1,0:T(8,128)(2,1)S(1)}, bf16[2,256,768]{2,1,0:T(8,128)(2,1)S(1)}, u32[]{:S(2)}, u32[]{:S(2)}) collective-permute-start(bf16[2,256,768]{2,1,0:T(8,128)(2,1)S(1)} %get-tuple-element.53), channel_id=1, source_target_pairs={{0,2},{2,0},{4,6},{6,4},{8,10},{10,8},{12,14},{14,12},{1,3},{3,1},... | collective-permute-start | bytes 2359304 | tf_op jit(solution)/shard_map/ppermute | solution.py:616
  143.8 36.1 %collective-permute-start.11 = (bf16[2,256,768]{2,1,0:T(8,128)(2,1)}, bf16[2,256,768]{2,1,0:T(8,128)(2,1)}, u32[]{:S(2)}, u32[]{:S(2)}) collective-permute-start(bf16[2,256,768]{2,1,0:T(8,128)(2,1)} %get-tuple-element.52), channel_id=1, source_target_pairs={{0,2},{2,0},{4,6},{6,4},{8,10},{10,8},{12,14},{14,12},{1,3},{3,1},... | collective-permute-start | bytes 2359304 | tf_op jit(solution)/shard_map/ppermute | solution.py:611
  146.4 70.3 %collective-permute-start.19 = (bf16[2,784,256]{2,1,0:T(8,128)(2,1)}, bf16[2,784,256]{2,1,0:T(8,128)(2,1)}, u32[]{:S(2)}, u32[]{:S(2)}) collective-permute-start(bf16[2,784,256]{2,1,0:T(8,128)(2,1)} %get-tuple-element.59), channel_id=1, source_target_pairs={{0,2},{2,0},{4,6},{6,4},{8,10},{10,8},{12,14},{14,12},{1,3},{3,1},... | collective-permute-start | bytes 2408456 | tf_op jit(solution)/shard_map/ppermute | solution.py:616
  150.9 63.1 %collective-permute-start.5 = (bf16[2,256,768]{2,1,0:T(8,128)(2,1)}, bf16[2,256,768]{2,1,0:T(8,128)(2,1)}, u32[]{:S(2)}, u32[]{:S(2)}) collective-permute-start(bf16[2,256,768]{2,1,0:T(8,128)(2,1)} %get-tuple-element.47), channel_id=1, source_target_pairs={{0,2},{2,0},{4,6},{6,4},{8,10},{10,8},{12,14},{14,12},{1,3},{3,1},... | collective-permute-start | bytes 2359304 | tf_op jit(solution)/shard_map/ppermute | solution.py:616
  154.4 72.4 %collective-permute-start.18 = (bf16[2,784,256]{2,1,0:T(8,128)(2,1)S(1)}, bf16[2,784,256]{2,1,0:T(8,128)(2,1)S(1)}, u32[]{:S(2)}, u32[]{:S(2)}) collective-permute-start(bf16[2,784,256]{2,1,0:T(8,128)(2,1)S(1)} %copy-done.52), channel_id=1, source_target_pairs={{0,2},{2,0},{4,6},{6,4},{8,10},{10,8},{12,14},{14,12},{1,3},{3,1},... | collective-permute-start | bytes 2408456 | tf_op jit(solution)/shard_map/ppermute | solution.py:611
  163.1 85.4 %collective-permute-start.14 = (bf16[2,256,1024]{2,1,0:T(8,128)(2,1)S(1)}, bf16[2,256,1024]{2,1,0:T(8,128)(2,1)S(1)}, u32[]{:S(2)}, u32[]{:S(2)}) collective-permute-start(bf16[2,256,1024]{2,1,0:T(8,128)(2,1)S(1)} %shard_map.198), channel_id=1, source_target_pairs={{0,16},{16,0},{1,17},{17,1},{2,18},{18,2},{3,19},{19,3},{4,20},{20... | collective-permute-start | bytes 3145736 | tf_op jit(solution)/shard_map/ppermute | solution.py:618
  181.1 52.0 %collective-permute-start.13 = (bf16[1,256,1792]{2,1,0:T(8,128)(2,1)S(1)}, bf16[1,256,1792]{2,1,0:T(8,128)(2,1)S(1)}, u32[]{:S(2)}, u32[]{:S(2)}) collective-permute-start(bf16[1,256,1792]{2,1,0:T(8,128)(2,1)S(1)} %shard_map.197), channel_id=1, source_target_pairs={{0,16},{16,0},{1,17},{17,1},{2,18},{18,2},{3,19},{19,3},{4,20},{20... | collective-permute-start | bytes 2752520 | tf_op jit(solution)/shard_map/ppermute | solution.py:614
  216.8 31.7 %collective-permute-start.7 = (bf16[2,256,768]{2,1,0:T(8,128)(2,1)S(1)}, bf16[2,256,768]{2,1,0:T(8,128)(2,1)S(1)}, u32[]{:S(2)}, u32[]{:S(2)}) collective-permute-start(bf16[2,256,768]{2,1,0:T(8,128)(2,1)S(1)} %shard_map.194), channel_id=1, source_target_pairs={{0,16},{16,0},{1,17},{17,1},{2,18},{18,2},{3,19},{19,3},{4,20},{20... | collective-permute-start | bytes 2359304 | tf_op jit(solution)/shard_map/ppermute | solution.py:618
  226.9 48.8 %collective-permute-start.21 = (bf16[2,896,256]{2,1,0:T(8,128)(2,1)S(1)}, bf16[2,896,256]{2,1,0:T(8,128)(2,1)S(1)}, u32[]{:S(2)}, u32[]{:S(2)}) collective-permute-start(bf16[2,896,256]{2,1,0:T(8,128)(2,1)S(1)} %shard_map.204), channel_id=1, source_target_pairs={{0,16},{16,0},{1,17},{17,1},{2,18},{18,2},{3,19},{19,3},{4,20},{20... | collective-permute-start | bytes 2752520 | tf_op jit(solution)/shard_map/ppermute | solution.py:618
  231.6 44.1 %collective-permute-start.20 = (bf16[1,1536,256]{2,1,0:T(8,128)(2,1)S(1)}, bf16[1,1536,256]{2,1,0:T(8,128)(2,1)S(1)}, u32[]{:S(2)}, u32[]{:S(2)}) collective-permute-start(bf16[1,1536,256]{2,1,0:T(8,128)(2,1)S(1)} %shard_map.203), channel_id=1, source_target_pairs={{0,16},{16,0},{1,17},{17,1},{2,18},{18,2},{3,19},{19,3},{4,20},{20... | collective-permute-start | bytes 2359304 | tf_op jit(solution)/shard_map/ppermute | solution.py:614
  233.2 51.2 %collective-permute-start.24 = (bf16[2,256,768]{2,1,0:T(8,128)(2,1)S(1)}, bf16[2,256,768]{2,1,0:T(8,128)(2,1)S(1)}, u32[]{:S(2)}, u32[]{:S(2)}) collective-permute-start(bf16[2,256,768]{2,1,0:T(8,128)(2,1)S(1)} %get-tuple-element.61), channel_id=1, source_target_pairs={{4,8},{6,10},{8,4},{10,6},{5,9},{7,11},{9,5},{11,7},{20,24},{22,26... | collective-permute-start | bytes 2359304 | tf_op jit(solution)/shard_map/ppermute | solution.py:610
  284.2 72.7 %collective-permute-start.22 = (bf16[640,2048]{1,0:T(8,128)(2,1)}, bf16[640,2048]{1,0:T(8,128)(2,1)}, u32[]{:S(2)}, u32[]{:S(2)}) collective-permute-start(bf16[640,2048]{1,0:T(8,128)(2,1)} %shard_map.205.refs_3_), channel_id=1, source_target_pairs={{0,1},{1,0},{2,3},{3,2},{4,5},{5,4},{6,7},{7,6},{8,9},{9,8},{10,11... | collective-permute-start | bytes 7864328 | tf_op jit(solution)/shard_map/ppermute | solution.py:665
  284.3 21.8 %collective-permute-start.25 = (bf16[2,256,768]{2,1,0:T(8,128)(2,1)S(1)}, bf16[2,256,768]{2,1,0:T(8,128)(2,1)S(1)}, u32[]{:S(2)}, u32[]{:S(2)}) collective-permute-start(bf16[2,256,768]{2,1,0:T(8,128)(2,1)S(1)} %collective-permute-done.24.m_ref), channel_id=1, source_target_pairs={{4,0},{6,2},{8,12},{10,14},{5,1},{7,3},{9,13},{11,15},{20,16},{22,... | collective-permute-start | bytes 2359304 | tf_op jit(solution)/shard_map/ppermute | solution.py:612
  308.5 22.5 %collective-permute-start.26 = (bf16[2,256,512]{2,1,0:T(8,128)(2,1)S(1)}, bf16[2,256,512]{2,1,0:T(8,128)(2,1)S(1)}, u32[]{:S(2)}, u32[]{:S(2)}) collective-permute-start(bf16[2,256,512]{2,1,0:T(8,128)(2,1)S(1)} %get-tuple-element.64), channel_id=1, source_target_pairs={{0,2},{2,0},{4,6},{6,4},{8,10},{10,8},{12,14},{14,12},{1,3},{3,1},... | collective-permute-start | bytes 1572872 | tf_op jit(solution)/shard_map/ppermute | solution.py:611
  322.1 34.8 %collective-permute-start.29 = (bf16[2,256,768]{2,1,0:T(8,128)(2,1)}, bf16[2,256,768]{2,1,0:T(8,128)(2,1)}, u32[]{:S(2)}, u32[]{:S(2)}) collective-permute-start(bf16[2,256,768]{2,1,0:T(8,128)(2,1)} %shard_map.210), channel_id=1, source_target_pairs={{0,16},{16,0},{1,17},{17,1},{2,18},{18,2},{3,19},{19,3},{4,20},{20... | collective-permute-start | bytes 2359304 | tf_op jit(solution)/shard_map/ppermute | solution.py:618
  331.9 25.0 %collective-permute-start.28 = (bf16[1,256,1280]{2,1,0:T(8,128)(2,1)}, bf16[1,256,1280]{2,1,0:T(8,128)(2,1)}, u32[]{:S(2)}, u32[]{:S(2)}) collective-permute-start(bf16[1,256,1280]{2,1,0:T(8,128)(2,1)} %shard_map.209), channel_id=1, source_target_pairs={{0,16},{16,0},{1,17},{17,1},{2,18},{18,2},{3,19},{19,3},{4,20},{20... | collective-permute-start | bytes 1966088 | tf_op jit(solution)/shard_map/ppermute | solution.py:614
  343.1 25.6 %collective-permute-start.36 = (bf16[1,640,256]{2,1,0:T(8,128)(2,1)S(1)}, bf16[1,640,256]{2,1,0:T(8,128)(2,1)S(1)}, u32[]{:S(2)}, u32[]{:S(2)}) collective-permute-start(bf16[1,640,256]{2,1,0:T(8,128)(2,1)S(1)} %shard_map.215), channel_id=1, source_target_pairs={{0,16},{16,0},{1,17},{17,1},{2,18},{18,2},{3,19},{19,3},{4,20},{20... | collective-permute-start | bytes 983048 | tf_op jit(solution)/shard_map/ppermute | solution.py:614
  (85 other events, 2250.8 us)
